TPU v7x, 512 devices: a whole 4x4x16 slice. The times are simulated.
512 devices in a mesh: ep: 16 (over y, x), tp: 32 (over z, core).
Axes of the slice: x: 4, y: 4, z: 16, core: 2. Of those that a mesh axis runs over, the one named last changes fastest.
Arguments:
- tokens: bfloat16 [4096, 2048], P('ep'), may hold values from -6 to 6
- cotangent: bfloat16 [4096, 2048], P('ep'), may hold values from -6 to 6
- group_prob: float32 [4096], P('ep'), may hold values from 0.25 to 1
- expert_prob: float32 [4096, 2], P('ep'), may hold values from 0.1 to 1
- routing: int32 [4096, 2], P('ep'), may hold values from 0 to 15, all different within a row; in each aligned block of 256 rows (0 to 255, 256 to 511, ...) at most 48 rows name the same one
- gate_weight: bfloat16 [16, 2048, 4096], P('ep', None, 'tp'), may hold values from -0.125 to 0.125
- up_weight: bfloat16 [16, 2048, 4096], P('ep', None, 'tp'), may hold values from -0.125 to 0.125
- down_weight: bfloat16 [16, 4096, 2048], P('ep', 'tp'), may hold values from -1 to 1
Outputs:
- token_grad: bfloat16 [4096, 2048], P('ep')
- group_prob_grad: float32 [4096], P('ep')
- expert_prob_grad: float32 [4096, 2], P('ep')
- gate_weight_grad: bfloat16 [16, 2048, 4096], P('ep', None, 'tp')
- up_weight_grad: bfloat16 [16, 2048, 4096], P('ep', None, 'tp')
- down_weight_grad: bfloat16 [16, 4096, 2048], P('ep', 'tp')
- gate_row_norms: float32 [16, 2048], P('ep')
- up_row_norms: float32 [16, 2048], P('ep')
- down_row_norms: float32 [16, 4096], P('ep', 'tp')
Inputs may be any that keep to these rules, and one draw needn't show every extreme that they name: `routing`: each row names 2 different experts. In each aligned block of 256 rows no expert is named by more than 48 rows, and in every draw some expert is named by exactly 48 rows of some block.
All inputs are finite; a program needn't handle non-finite values.
Results may differ from a plain program's by a relative error of at most 0.0065.
Values may be sent and summed in bfloat16 or wider, within the bound.
A program may use at most 64 MiB of HBM per device.

v0:
```python
import jax
import jax.numpy as jnp
from jax import lax
from jax.sharding import PartitionSpec as P


def side_by_side(arrays, axis, split_dim, concat_dim, along):
    both = jnp.concatenate(arrays, axis=along)
    whole, at, finished = (
        lax.all_to_all(both, axis, split_axis=split_dim, concat_axis=concat_dim, tiled=True),
        0,
        [],
    )
    for a in arrays:
        finished.append(lax.slice_in_dim(whole, at, at + a.shape[along], axis=along))
        at += a.shape[along]
    return tuple(finished)


def slot_targets(route_block, expert_count, capacity):
    flat = route_block.reshape(-1)
    names = jnp.arange(expert_count, dtype=jnp.int32)
    onehot = (flat[:, None] == names[None, :]).astype(jnp.int32)
    before = jnp.cumsum(onehot, axis=0) - onehot
    place = jnp.sum(before * onehot, axis=1)
    return flat * capacity + place


def local(tokens, cotangent, group_prob, expert_prob, routing, gate_weight, up_weight, down_weight):
    tok_count, model_width = tokens.shape
    top_count = routing.shape[1]
    expert_count = lax.axis_size("ep")
    capacity = 3 * tok_count * top_count // (2 * expert_count)
    slot_count = tok_count * top_count
    buffer_rows = expert_count * capacity
    target = slot_targets(routing, expert_count, capacity)
    weight = group_prob[:, None] * expert_prob
    flat_weight = weight.reshape(slot_count)
    owner = (
        jnp.full((buffer_rows,), slot_count, jnp.int32)
        .at[target]
        .set(jnp.arange(slot_count, dtype=jnp.int32))
    )
    filled = owner < slot_count
    safe_slot = jnp.minimum(owner, slot_count - 1)
    source = safe_slot // top_count
    send_in = jnp.where(filled[:, None], tokens[source], jnp.zeros((), jnp.bfloat16))
    send_in = send_in.reshape(expert_count, capacity, model_width)
    scaled = flat_weight[safe_slot][:, None] * cotangent[source].astype(jnp.float32)
    send_scaled = jnp.where(filled[:, None], scaled, 0.0).astype(jnp.bfloat16)
    send_scaled = send_scaled.reshape(expert_count, capacity, model_width)
    rows_in, rows_scaled = side_by_side((send_in, send_scaled), "ep", 0, 0, 1)
    flat_in = rows_in.reshape(buffer_rows, model_width)
    flat_scaled = rows_scaled.reshape(buffer_rows, model_width)
    w_gate = gate_weight[0]
    w_up = up_weight[0]
    w_down = down_weight[0]
    hidden_total = gate_weight.shape[2] * lax.axis_size("tp")
    contract_last = (((1,), (1,)), ((), ()))
    contract_rows = (((0,), (0,)), ((), ()))
    pre_gate = jnp.dot(flat_in, w_gate, preferred_element_type=jnp.float32)
    pre_up = jnp.dot(flat_in, w_up, preferred_element_type=jnp.float32)
    sigma = jax.nn.sigmoid(pre_gate)
    activated = pre_gate * sigma
    derivative = sigma * (1.0 + pre_gate * (1.0 - sigma))
    hidden = (activated * pre_up).astype(jnp.bfloat16)
    hidden_grad = lax.dot_general(
        flat_scaled, w_down, contract_last, preferred_element_type=jnp.float32
    )
    score_part = jnp.sum(hidden.astype(jnp.float32) * hidden_grad, axis=1).reshape(
        expert_count, capacity
    )
    gate_pre = (hidden_grad * pre_up * derivative).astype(jnp.bfloat16)
    up_pre = (hidden_grad * activated).astype(jnp.bfloat16)
    down_sum = lax.dot_general(
        hidden, flat_scaled, contract_rows, preferred_element_type=jnp.float32
    )
    gate_sum = lax.dot_general(flat_in, gate_pre, contract_rows, preferred_element_type=jnp.float32)
    up_sum = lax.dot_general(flat_in, up_pre, contract_rows, preferred_element_type=jnp.float32)
    input_part = lax.dot_general(
        gate_pre, w_gate, contract_last, preferred_element_type=jnp.float32
    )
    input_part = input_part + lax.dot_general(
        up_pre, w_up, contract_last, preferred_element_type=jnp.float32
    )
    input_part = input_part.reshape(expert_count, capacity, model_width)
    norm_part = (
        jnp.stack([jnp.sum(gate_sum * gate_sum, axis=1), jnp.sum(up_sum * up_sum, axis=1)])
        / hidden_total
    )
    down_norms = jnp.sum(down_sum * down_sum, axis=1) / model_width
    summed, scores, row_norms = lax.psum((input_part, score_part, norm_part), "tp")
    returned_rows = lax.all_to_all(
        summed.astype(jnp.bfloat16), "ep", split_axis=0, concat_axis=0, tiled=True
    )
    returned_scores = lax.all_to_all(scores, "ep", split_axis=0, concat_axis=0, tiled=True)
    per_slot = returned_rows.reshape(buffer_rows, model_width)[target]
    per_slot = per_slot.astype(jnp.float32).reshape(tok_count, top_count, model_width)
    token_grad = jnp.sum(per_slot, axis=1).astype(jnp.bfloat16)
    slot_score = returned_scores.reshape(buffer_rows)[target].reshape(tok_count, top_count) / weight
    expert_prob_grad = group_prob[:, None] * slot_score
    group_prob_grad = jnp.sum(expert_prob * slot_score, axis=1)
    return (
        token_grad,
        group_prob_grad,
        expert_prob_grad,
        gate_sum.astype(jnp.bfloat16)[None],
        up_sum.astype(jnp.bfloat16)[None],
        down_sum.astype(jnp.bfloat16)[None],
        row_norms[0][None],
        row_norms[1][None],
        down_norms[None],
    )


def solution(mesh):
    return jax.shard_map(
        local,
        mesh=mesh,
        in_specs=(
            P("ep", None),
            P("ep", None),
            P("ep"),
            P("ep", None),
            P("ep", None),
            P("ep", None, "tp"),
            P("ep", None, "tp"),
            P("ep", "tp", None),
        ),
        out_specs=(
            P("ep", None),
            P("ep"),
            P("ep", None),
            P("ep", None, "tp"),
            P("ep", None, "tp"),
            P("ep", "tp", None),
            P("ep", None),
            P("ep", None),
            P("ep", "tp"),
        ),
        check_vma=False,
    )
```

profile of v0, /device:TPU:96, one launch (start us, length us, event | category | flops | bytes accessed | tf_op | source)
XLA Modules:
  0.0 325.9 jit_solution(3121891964003576167)
XLA Ops:
  0.7 0.8 broadcast_multiply_fusion.2
  1.4 0.8 copy.20
  2.8 1.2 reduce-window.6
  4.4 2.4 scatter_custom_fusion
  6.9 0.8 copy.23
  7.8 0.8 broadcast_multiply_fusion.1
  8.7 5.0 %gather_fusion.1 = f32[768]{0:T(1024)S(1)} fusion(f32[512]{0:T(512)S(1)} %reshape.126, s32[1024]{0:T(1024)S(1)} %get-tuple-element.48), kind=kCustom, calls=%fused_computation.1 | custom fusion | bytes 9216 | tf_op jit(solution)/shard_map/gather | solution.py:49
  13.8 4.3 %gather_fusion.2 = bf16[768,2048]{1,0:T(8,128)(2,1)} fusion(bf16[256,2048]{1,0:T(8,128)(2,1)S(1)} %copy-done, s32[1024]{0:T(1024)S(1)} %get-tuple-element.49), kind=kCustom, calls=%fused_computation.2 | custom fusion | bytes 6294528 | tf_op jit(solution)/shard_map/gather | solution.py:49
  18.1 4.3 %gather_fusion = bf16[768,2048]{1,0:T(8,128)(2,1)} fusion(bf16[256,2048]{1,0:T(8,128)(2,1)S(1)} %copy-done.1, s32[1024]{0:T(1024)S(1)} %get-tuple-element.49), kind=kCustom, calls=%fused_computation | custom fusion | bytes 6294528 | tf_op jit(solution)/shard_map/gather | solution.py:47
  22.4 2.3 broadcast_select_fusion
  25.2 2.5 fusion.1
  27.7 3.0 pad_maximum_fusion
  30.7 80.2 %all_to_all.19 = bf16[16,96,2048]{2,1,0:T(8,128)(2,1)S(1)} all-to-all(bf16[16,96,2048]{2,1,0:T(8,128)(2,1)S(1)} %pad_maximum_fusion), channel_id=1, replica_groups=mesh['ep'=16,'tp'=32] {'ep'}, dimensions={0} | all-to-all | bytes 12582912 | tf_op jit(solution)/shard_map/all_to_all | solution.py:10
  110.8 1.1 fusion.20
  112.0 1.2 fusion.4
  113.4 1.2 fusion.7
  114.6 1.2 multiply_reduce_fusion.3
  116.5 3.7 %fusion.2 = f32[768,2048]{1,0:T(8,128)} fusion(bf16[768,128]{0,1:T(8,128)(2,1)S(1)} %get-tuple-element.34, bf16[1,2048,128]{2,1,0:T(8,128)(2,1)S(1)} %copy-done.5), kind=kOutput, calls=%fused_computation.15 | convolution fusion | flops 402653184 | bytes 7012352 | tf_op jit(solution)/shard_map/dot_general | solution.py:80
  120.3 2.5 convert_bitcast_fusion.1
  122.8 6.5 %convolution_add_fusion = f32[768,2048]{1,0:T(8,128)} fusion(f32[768,2048]{1,0:T(8,128)} %fusion.2, bf16[768,128]{0,1:T(8,128)(2,1)S(1)} %get-tuple-element.41, bf16[1,2048,128]{2,1,0:T(8,128)(2,1)S(1)} %copy-done.6), kind=kOutput, calls=%fused_computation.10 | convolution fusion | flops 404226048 | bytes 13303808 | tf_op jit(solution)/shard_map/dot_general | solution.py:83
  129.2 116.7 %all-reduce.2 = (bf16[16,48,2048]{2,1,0:T(8,128)(2,1)}, f32[16,1,48]{2,1,0:T(1,128)S(1)}, f32[2,2048]{1,0:T(2,128)S(1)}) all-reduce(f32[16,48,2048]{2,1,0:T(8,128)} %bitcast.69, f32[16,1,48]{2,1,0:T(1,128)S(1)} %all_to_all.14, f32[2,2048]{1,0:T(2,128)S(1)} %maximum_multiply_fusion), channel_id=1, replica_groups=mesh['ep'=16,'tp'=32] {'tp'}, use_global_device_ids=true, to_apply=%region_4.5 | all-reduce | flops 1577728 | bytes 9476096 | tf_op jit(solution)/shard_map/psum | solution.py:92
  245.9 10.5 %all_to_all.20 = f32[16,1,48]{2,1,0:T(1,128)S(1)} all-to-all(f32[16,1,48]{2,1,0:T(1,128)S(1)} %get-tuple-element.28), channel_id=1, replica_groups=mesh['ep'=16,'tp'=32] {'ep'}, dimensions={0} | all-to-all | bytes 6144 | tf_op jit(solution)/shard_map/all_to_all | solution.py:96
  256.5 4.7 %all-to-all-start.1 = ((bf16[16,48,2048]{2,1,0:T(8,128)(2,1)}), bf16[16,48,2048]{2,1,0:T(8,128)(2,1)}, u32[]{:S(2)}, u32[]{:S(2)}) async-start(bf16[16,48,2048]{2,1,0:T(8,128)(2,1)} %get-tuple-element.27), calls=%async_computation.1 | async-start | bytes 6291456 | tf_op jit(solution)/shard_map/all_to_all | solution.py:93
  261.2 1.0 copy.27
  262.2 1.0 copy.26
  263.2 3.3 %multiply_reduce_fusion = (f32[128]{0:T(128)S(1)}, bf16[1,128,2048]{2,1,0:T(8,128)(2,1)}) fusion(bf16[768,128]{0,1:T(8,128)(2,1)S(1)} %get-tuple-element.31, bf16[768,2048]{1,0:T(8,128)(2,1)} %bitcast.71), kind=kOutput, calls=%fused_computation.12 | convolution fusion | flops 403439488 | bytes 3867136 | tf_op jit(solution)/shard_map/dot_general | solution.py:75
  268.9 2.3 gather_fusion.4
  271.3 0.8 broadcast_multiply_fusion
  272.7 36.1 %all-to-all-done.1 = bf16[16,48,2048]{2,1,0:T(8,128)(2,1)} async-done(((bf16[16,48,2048]{2,1,0:T(8,128)(2,1)}), bf16[16,48,2048]{2,1,0:T(8,128)(2,1)}, u32[]{:S(2)}, u32[]{:S(2)}) %all-to-all-start.1) | async-done | bytes 3145760 | tf_op jit(solution)/shard_map/all_to_all | solution.py:93
  308.8 6.7 %gather_fusion.3 = bf16[512,2048]{1,0:T(8,128)(2,1)S(1)} fusion(bf16[768,2048]{1,0:T(8,128)(2,1)} %bitcast.11, s32[1024]{0:T(1024)S(1)} %pad_clamp_fusion), kind=kCustom, calls=%fused_computation.3 | custom fusion | bytes 4196352 | tf_op jit(solution)/shard_map/gather | solution.py:97
  315.5 2.7 gather.24
  318.2 7.7 %reduce_sum.70 = bf16[256,2048]{1,0:T(8,128)(2,1)} reduce(bf16[256,2,2048]{2,1,0:T(2,128)(2,1)} %gather.24, bf16[]{:T(256)} %constant.39.clone.1), dimensions={1}, to_apply=%region_5.6 | reduce | flops 524288 | bytes 3145730 | tf_op jit(solution)/shard_map/reduce_sum | solution.py:99
  (46 shorter events, 5.9 us)
Async XLA Ops:
  0.6 13.2 %copy-start = (bf16[256,2048]{1,0:T(8,128)(2,1)S(1)}, bf16[256,2048]{1,0:T(8,128)(2,1)}, u32[]{:S(2)}) copy-start(bf16[256,2048]{1,0:T(8,128)(2,1)} %param.9) | copy-start | bytes 3145732
  13.8 4.3 %copy-start.1 = (bf16[256,2048]{1,0:T(8,128)(2,1)S(1)}, bf16[256,2048]{1,0:T(8,128)(2,1)}, u32[]{:S(2)}) copy-start(bf16[256,2048]{1,0:T(8,128)(2,1)} %param.8) | copy-start | bytes 3145732
  22.4 2.8 copy-start.4
  110.8 1.2 copy-start.5
  112.0 2.6 copy-start.3
  112.0 3.9 %copy-start.2 = (bf16[16,48,2048]{2,1,0:T(8,128)(2,1)}, bf16[16,48,2048]{2,1,0:T(8,128)(2,1)S(1)}, u32[]{:S(2)}) copy-start(bf16[16,48,2048]{2,1,0:T(8,128)(2,1)S(1)} %get-tuple-element.33) | copy-start | bytes 9437188
  112.0 1.4 copy-start.6
  112.0 2.6 copy-start.8
  256.5 52.4 %all-to-all-start.1 = ((bf16[16,48,2048]{2,1,0:T(8,128)(2,1)}), bf16[16,48,2048]{2,1,0:T(8,128)(2,1)}, u32[]{:S(2)}, u32[]{:S(2)}) async-start(bf16[16,48,2048]{2,1,0:T(8,128)(2,1)} %get-tuple-element.27), calls=%async_computation.1 | async-start | bytes 6291456 | tf_op jit(solution)/shard_map/all_to_all | solution.py:93
  263.2 8.1 %copy-start.7 = (f32[256]{0:T(256)S(1)}, f32[256]{0:T(256)}, u32[]{:S(2)}) copy-start(f32[256]{0:T(256)} %param.10) | copy-start | bytes 3076
where the time goes:
time: 326 us
  blocking collectives  207 us (63%)
  local copies, waits for them, and re-layouts  36.3 us (11%)
  waiting for transfers between devices  36.1 us (11%)
  other arithmetic  20.3 us (6%)
  matrix products  20.1 us (6%)
  starting transfers between devices  4.7 us (1%)
    psum x1, blocking collectives, local(): lax.psum((input_part, score_part, norm_part), 'tp')  117 us
    all_to_all x1, blocking collectives, side_by_side(): lax.all_to_all(both, axis, split_axis=split_dim, concat_axis=concat_dim,...  80.2 us
    all_to_all x1, waiting for transfers between devices, local(): lax.all_to_all(summed.astype(jnp.bfloat16), 'ep', split_axis=0, concat_ax...  36.1 us
    all_to_all x1, blocking collectives, local(): lax.all_to_all(scores, 'ep', split_axis=0, concat_axis=0, tiled=True)  10.5 us
    gather x2, local copies, waits for them, and re-layouts, local(): per_slot = returned_rows.reshape(buffer_rows, model_width)[target]  9.37 us
    reduce_sum x1, other arithmetic, local(): token_grad = jnp.sum(per_slot, axis=1).astype(jnp.bfloat16)  7.65 us
  transfers between devices with their start and end apart: 1, of which 1 were waited for; matrix products, arithmetic and copies ran while one was open for 4% of the time, Pallas kernels for 0%

commit v1 on v0

v1 whole, which is shorter than its diff:
```python
import functools
import jax
import jax.numpy as jnp
from jax import lax
from jax.experimental import pallas as pl
from jax.experimental.pallas import tpu as pltpu
from jax.sharding import PartitionSpec as P

MESH = pl.DeviceIdType.MESH
LANES = 128
F32 = jnp.float32
BF16 = jnp.bfloat16
CONTRACT_LAST = (((1,), (1,)), ((), ()))


def plane_peer(e, j, n_ep):
    if n_ep == 16:
        y, x = e // 4, e % 4
        return ((y + j // 4) % 4) * 4 + (x + j % 4) % 4
    return (e + j) % n_ep


def plane_source(e, j, n_ep):
    if n_ep == 16:
        y, x = e // 4, e % 4
        return ((y + 4 - j // 4) % 4) * 4 + (x + 4 - j % 4) % 4
    return (e + n_ep - j) % n_ep


def slot_rows(r, n_ep, cap):
    tok = r.shape[1]
    names = lax.broadcasted_iota(jnp.int32, (n_ep, tok), 0)
    first = (names == r[0:1, :]).astype(F32)
    second = (names == r[1:2, :]).astype(F32)
    earlier = lax.broadcasted_iota(jnp.int32, (tok, tok), 0) < lax.broadcasted_iota(
        jnp.int32, (tok, tok), 1
    )
    before = jnp.dot(
        (first + second).astype(BF16),
        jnp.where(earlier, 1.0, 0.0).astype(BF16),
        preferred_element_type=F32,
    )
    out = []
    for k, hot in enumerate((first, second)):
        place = jnp.sum(hot * before, axis=0, keepdims=True)
        out.append(r[k : k + 1, :].astype(F32) * float(cap) + place)
    return out


def body(
    n_ep, n_z, cap,
    r_ref, gp_ref, ep_ref, tok_hbm, cot_hbm, wg_hbm, wu_hbm, wd_hbm,
    tg_out, gg_out, ug_out, dg_out, gn_out, un_out, dn_out, epg_out, gpg_out,
    x, send, rows, wgu, wd, pre, hg, gpu, gput, hidt, prod,
    own, sib_send, sib_recv, dn_send, dn_recv, up_send, up_recv,
    sc_send, sc_recv, sm, sm_recv, sm_tot, sm_sib, sm_fin,
    fin, gat, tg, gg, ug, dg, dnacc,
    ld_sem, wl_sem, loc_sem, in_s, in_r, za_s, za_r, zb_s, zb_r, dx_s, dx_r, dy_s, dy_r,
    sc_s, sc_r, pt_s, pt_r, rd_s, rd_r, ru_s, ru_r, ms_s, ms_r, mx_s, mx_r, mg_s, mg_r,
    fa_s, fa_r, au_s, au_r, ad_s, ad_r, as_s, as_r, out_sem,
):
    e, tp = lax.axis_index("ep"), lax.axis_index("tp")
    z, c = tp // 2, tp % 2
    par = z % 2
    mine, other = par * 2, 2 - par * 2
    near, far = z + 1 - 2 * par, (z + n_z - 1 + 2 * par) % n_z
    up_z, dn_z = (z + 1) % n_z, (z + n_z - 1) % n_z
    tok, quarter = x.shape[0], rows.shape[3]
    slots = n_ep * cap
    half = slots // 2
    nd, nu = n_z // 2, n_z // 2 - 1
    qc = quarter // LANES
    sibling = (e, z * 2 + 1 - c)

    def at_z(other_z):
        return (e, other_z * 2 + c)

    def remote(src, dst, s_sem, r_sem, dev):
        return pltpu.make_async_remote_copy(
            src_ref=src, dst_ref=dst, send_sem=s_sem, recv_sem=r_sem,
            device_id=dev, device_id_type=MESH,
        )

    barrier = pltpu.get_barrier_semaphore()

    @pl.loop(1, n_ep)
    def _(j):
        pl.semaphore_signal(
            barrier, inc=1, device_id=(plane_peer(e, j, n_ep), tp), device_id_type=MESH
        )

    @pl.loop(1, n_z)
    def _(j):
        pl.semaphore_signal(barrier, inc=1, device_id=at_z((z + j) % n_z), device_id_type=MESH)

    pl.semaphore_signal(barrier, inc=1, device_id=sibling, device_id_type=MESH)

    start_col = pl.multiple_of(par * (2 * quarter), LANES)

    @pl.when(c == 0)
    def _():
        pltpu.make_async_copy(tok_hbm.at[:, pl.ds(start_col, 2 * quarter)], x, ld_sem).start()

    @pl.when(c == 1)
    def _():
        pltpu.make_async_copy(cot_hbm.at[:, pl.ds(start_col, 2 * quarter)], x, ld_sem).start()

    def weight_loads():
        out = []
        for q in range(4):
            span = pl.ds(q * quarter, quarter)
            out.append((wg_hbm.at[0, span, :], wgu.at[q, :, pl.ds(0, LANES)], wl_sem.at[q, 0]))
            out.append((wu_hbm.at[0, span, :], wgu.at[q, :, pl.ds(LANES, LANES)], wl_sem.at[q, 1]))
            out.append((wd_hbm.at[0, :, span], wd.at[q], wl_sem.at[q, 2]))
        return [pltpu.make_async_copy(*args) for args in out]

    for copy in weight_loads():
        copy.start()

    r = r_ref[...]
    weight = gp_ref[...] * ep_ref[...]
    w_eff = jnp.where(c == 0, jnp.ones_like(weight), weight)
    slot0, slot1 = slot_rows(r, n_ep, cap)
    pltpu.make_async_copy(tok_hbm.at[:, pl.ds(start_col, 2 * quarter)], x, ld_sem).wait()

    @pl.loop(0, slots // LANES)
    def _(i):
        at = pl.multiple_of(i * LANES, LANES)
        here = (lax.broadcasted_iota(jnp.int32, (LANES, tok), 0) + at).astype(F32)
        m0, m1 = here == slot0, here == slot1
        pick = jnp.where(m0 | m1, 1.0, 0.0).astype(BF16)
        scale = jnp.sum(
            jnp.where(m0, w_eff[0:1, :], 0.0) + jnp.where(m1, w_eff[1:2, :], 0.0),
            axis=1, keepdims=True,
        )
        got = scale * jnp.dot(pick, x[...], preferred_element_type=F32)
        send[0, pl.ds(at, LANES), :] = got[:, :quarter].astype(BF16)
        send[1, pl.ds(at, LANES), :] = got[:, quarter:].astype(BF16)

    pl.semaphore_wait(barrier, n_ep - 1 + n_z - 1 + 1)

    def block(b):
        return pl.ds(pl.multiple_of(b * cap, 16), cap)

    def own_block():
        return pltpu.make_async_copy(
            send.at[:, block(e), :], rows.at[c, pl.ds(mine, 2), block(e), :], loc_sem.at[0]
        )

    def in_copy(src_block, to, sender):
        return remote(
            send.at[:, block(src_block), :], rows.at[c, pl.ds(mine, 2), block(sender), :],
            in_s.at[src_block], in_r.at[sender], (to, tp),
        )

    def za_copy(s, first):
        ref = rows.at[c, first, block(s), :]
        return remote(ref, ref, za_s.at[s], za_r.at[s], at_z(near))

    def zb_copy(s, first):
        ref = rows.at[c, first + 1, block(s), :]
        return remote(ref, ref, zb_s.at[s], zb_r.at[s], at_z(far))

    def dx_copy(s, arr):
        ref = rows.at[arr, pl.ds(mine, 2), block(s), :]
        return remote(ref, ref, dx_s.at[s], dx_r.at[s], sibling)

    def dy_copy(s, arr):
        ref = rows.at[arr, pl.ds(other, 2), block(s), :]
        return remote(ref, ref, dy_s.at[s], dy_r.at[s], sibling)

    own_block().start()

    @pl.loop(1, n_ep)
    def _(j):
        p = plane_peer(e, j, n_ep)
        in_copy(p, p, e).start()

    own_block().wait()
    za_copy(e, mine).start()
    zb_copy(e, mine).start()
    dx_copy(e, c).start()

    @pl.loop(1, n_ep)
    def _(j):
        s = plane_source(e, j, n_ep)
        in_copy(s, s, s).wait_recv()
        za_copy(s, mine).start()
        zb_copy(s, mine).start()
        dx_copy(s, c).start()

    @pl.loop(0, n_ep)
    def _(j):
        s = plane_source(e, j, n_ep)
        za_copy(s, other).wait_recv()
        zb_copy(s, other).wait_recv()
        dy_copy(s, c).start()

    for copy in weight_loads():
        copy.wait()

    @pl.loop(0, n_ep)
    def _(j):
        s = plane_source(e, j, n_ep)
        dx_copy(s, 1 - c).wait_recv()
        dy_copy(s, 1 - c).wait_recv()

    pre[...] = jnp.zeros_like(pre)
    hg[...] = jnp.zeros_like(hg)

    @pl.loop(0, 4)
    def _(q):
        pre[...] += jnp.dot(rows[0, q], wgu[q], preferred_element_type=F32)
        hg[...] += lax.dot_general(rows[1, q], wd[q], CONTRACT_LAST, preferred_element_type=F32)

    @pl.loop(0, slots // LANES)
    def _(i):
        at = pl.ds(pl.multiple_of(i * LANES, LANES), LANES)
        gate, upv, grad = pre[at, :LANES], pre[at, LANES:], hg[at, :]
        sigma = jax.nn.sigmoid(gate)
        activated = gate * sigma
        derivative = sigma * (1.0 + gate * (1.0 - sigma))
        hidden = (activated * upv).astype(BF16).astype(F32)
        gate_pre = (grad * upv * derivative).astype(BF16).astype(F32)
        up_pre = (grad * activated).astype(BF16).astype(F32)
        prod[at, :] = hidden * grad
        gpu[at, :LANES] = gate_pre.astype(BF16)
        gpu[at, LANES:] = up_pre.astype(BF16)
        gput[:LANES, at] = gate_pre.T.astype(BF16)
        gput[LANES:, at] = up_pre.T.astype(BF16)
        hidt[:, at] = hidden.T.astype(BF16)

    ones = jnp.ones((8, LANES), F32)
    for b in range(n_ep):
        row = lax.dot_general(
            ones, prod[b * cap : (b + 1) * cap, :], CONTRACT_LAST,
            precision=lax.Precision.HIGHEST, preferred_element_type=F32,
        )
        sc_send[b, :, :cap] = row[0:1, :]

    def sc_copy(to, sender):
        return remote(sc_send.at[to], sc_recv.at[sender], sc_s.at[to], sc_r.at[sender], (to, tp))

    @pl.loop(1, n_ep)
    def _(j):
        p = plane_peer(e, j, n_ep)
        sc_copy(p, e).start()

    keep = pl.ds(pl.multiple_of(c * half, 16), half)
    give = pl.ds(pl.multiple_of((1 - c) * half, 16), half)

    def pt_copy(o):
        return remote(sib_send.at[o], sib_recv.at[o], pt_s.at[o], pt_r.at[o], sibling)

    @pl.loop(0, 4)
    def _(q):
        given = lax.dot_general(gpu[give, :], wgu[q], CONTRACT_LAST, preferred_element_type=F32)
        for i in range(qc):
            sib_send[q * qc + i] = given[:, i * LANES : (i + 1) * LANES].astype(BF16)
        for i in range(qc):
            pt_copy(q * qc + i).start()
        kept = lax.dot_general(gpu[keep, :], wgu[q], CONTRACT_LAST, preferred_element_type=F32)
        for i in range(qc):
            own[q * qc + i] = kept[:, i * LANES : (i + 1) * LANES]

    dnacc[...] = jnp.zeros_like(dnacc)

    def weight_quarter(q):
        down = jnp.dot(hidt[...], rows[1, q], preferred_element_type=F32)
        dg[:, q * quarter : (q + 1) * quarter] = down.astype(BF16)
        square = down * down
        dnacc[...] += sum(square[:, i * LANES : (i + 1) * LANES] for i in range(qc))
        for k, target in enumerate((gg, ug)):
            both = jnp.dot(
                gput[k * LANES : (k + 1) * LANES, :], rows[0, q], preferred_element_type=F32
            )
            norm = jnp.sum(both * both, axis=0, keepdims=True)
            for i in range(qc):
                sm[q * qc + i, :, k * LANES : (k + 1) * LANES] = norm[:, i * LANES : (i + 1) * LANES]
            target[q * quarter : (q + 1) * quarter, :] = both.T.astype(BF16)

    def grad_stores():
        return [
            pltpu.make_async_copy(gg, gg_out.at[0], out_sem.at[0]),
            pltpu.make_async_copy(ug, ug_out.at[0], out_sem.at[1]),
            pltpu.make_async_copy(dg, dg_out.at[0], out_sem.at[2]),
        ]

    def own_scores():
        sc_recv[e] = sc_send[e]

    def ms_copy(o, sender):
        return remote(sm.at[o], sm_recv.at[sender], ms_s.at[o], ms_r.at[sender], at_z(o))

    def mx_copy():
        return remote(sm_tot, sm_sib, mx_s.at[0], mx_r.at[0], sibling)

    def mg_copy(piece, to):
        return remote(sm_fin.at[piece], sm_fin.at[piece], mg_s.at[to], mg_r.at[piece], at_z(to))

    score_rows = tok // LANES

    def small_start():
        own_scores()

        @pl.loop(1, n_ep)
        def _(j):
            s = plane_source(e, j, n_ep)
            sc_copy(s, s).wait_recv()

        got = sc_recv[...].reshape(n_ep, sc_recv.shape[2])
        fill = jnp.zeros((LANES - n_ep, got.shape[1]), F32)
        columns = jnp.concatenate([got, fill], axis=0).T
        totals = [jnp.zeros((1, tok), F32), jnp.zeros((1, tok), F32)]
        lane = lax.broadcasted_iota(jnp.int32, (cap, tok), 0)
        for s in range(n_ep):
            here = (lane + s * cap).astype(F32)
            column = columns[:cap, s : s + 1]
            for k, slot in enumerate((slot0, slot1)):
                totals[k] += jnp.sum(jnp.where(here == slot, column, 0.0), axis=0, keepdims=True)
        sm[:, :, 2 * LANES :] = jnp.zeros((n_z, 1, LANES), F32)
        for k in range(2):
            for h in range(score_rows):
                sm[k * score_rows + h, :, 2 * LANES :] = totals[k][:, h * LANES : (h + 1) * LANES]

        @pl.loop(1, n_z)
        def _(j):
            o = (z + j) % n_z
            ms_copy(o, z).start()

    def small_middle():
        @pl.loop(1, n_z)
        def _(j):
            s = (z + j) % n_z
            ms_copy(s, s).wait_recv()

        sm_recv[z] = sm[z]
        sm_tot[...] = jnp.sum(sm_recv[...], axis=0)
        mx_copy().start()

    def small_end():
        mx_copy().wait_recv()
        sm_fin[z] = sm_tot[...] + sm_sib[...]

        @pl.loop(1, n_z)
        def _(j):
            mg_copy(z, (z + j) % n_z).start()

    sub = half // 2

    def part(h):
        return pl.ds(h * sub, sub)

    def rd_copy(t, h):
        return remote(
            dn_send.at[t, part(h), :], dn_recv.at[t, part(h), :],
            rd_s.at[t, h], rd_r.at[t, h], at_z(dn_z),
        )

    def ru_copy(t, h):
        return remote(
            up_send.at[t, part(h), :], up_recv.at[t, part(h), :],
            ru_s.at[t, h], ru_r.at[t, h], at_z(up_z),
        )

    def chip_sum(o, h):
        return own[o, part(h), :] + sib_recv[o, part(h), :].astype(F32)

    for t in range(nd):
        o_dn, o_up = (z + n_z - nd + t) % n_z, (z + nu - t + n_z) % n_z
        pt_copy(o_dn).wait_recv()
        pt_copy(o_up).wait_recv()
        for h in range(2):
            total = chip_sum(o_dn, h)
            if t > 0:
                rd_copy(t - 1, h).wait_recv()
                total += dn_recv[t - 1, part(h), :].astype(F32)
            dn_send[t, part(h), :] = total.astype(BF16)
            rd_copy(t, h).start()
            if t < nu:
                total = chip_sum(o_up, h)
                if t > 0:
                    ru_copy(t - 1, h).wait_recv()
                    total += up_recv[t - 1, part(h), :].astype(F32)
                up_send[t, part(h), :] = total.astype(BF16)
                ru_copy(t, h).start()
        if n_z == 16:
            if t < 4:
                weight_quarter(t)
            if t == 3:
                small_start()
                for copy in grad_stores():
                    copy.start()
            if t == 6:
                small_middle()
        elif t == 0:
            for q in range(4):
                weight_quarter(q)
            small_start()
            for copy in grad_stores():
                copy.start()
            small_middle()

    for h in range(2):
        total = chip_sum(z, h)
        ru_copy(nu - 1, h).wait_recv()
        total += up_recv[nu - 1, part(h), :].astype(F32)
        rd_copy(nd - 1, h).wait_recv()
        total += dn_recv[nd - 1, part(h), :].astype(F32)
        fin[part(h), :] = total.astype(BF16)

    per_core = n_ep // 2
    ce = e // per_core

    def fa_copy(i, to, sender):
        return remote(
            fin.at[pl.ds(i * cap, cap), :], gat.at[block(sender), :],
            fa_s.at[i], fa_r.at[sender], (to, tp),
        )

    def fa_local(i):
        return pltpu.make_async_copy(
            fin.at[pl.ds(i * cap, cap), :], gat.at[block(e), :], loc_sem.at[1]
        )

    for i in range(per_core):
        b = c * per_core + i

        @pl.when(b != e)
        def _():
            fa_copy(i, b, e).start()

        @pl.when(b == e)
        def _():
            fa_local(i).start()

    small_end()

    def chunk(o):
        return tg.at[:, pl.ds(pl.multiple_of(o * LANES, LANES), LANES)]

    def au_copy(t, o):
        return remote(chunk(o), chunk(o), au_s.at[t], au_r.at[t], at_z(up_z))

    def ad_copy(t, o):
        return remote(chunk(o), chunk(o), ad_s.at[t], ad_r.at[t], at_z(dn_z))

    def as_copy(o):
        return remote(chunk(o), chunk(o), as_s.at[o], as_r.at[o], sibling)

    @pl.when(c == ce)
    def _():
        fa_local(0).wait()

        @pl.loop(1, n_ep)
        def _(j):
            s = (e + j) % n_ep
            fa_copy(0, s, s).wait_recv()

        acc = jnp.zeros((tok, LANES), F32)
        lane = lax.broadcasted_iota(jnp.int32, (slots, tok), 0).astype(F32)
        pick = jnp.where((lane == slot0) | (lane == slot1), 1.0, 0.0)
        acc = jnp.dot(pick.T.astype(BF16), gat[...], preferred_element_type=F32)
        tg[:, pl.ds(pl.multiple_of(z * LANES, LANES), LANES)] = acc.astype(BF16)
        au_copy(1, z).start()
        ad_copy(1, z).start()
        as_copy(z).start()
        for t in range(1, nd + 1):
            if t <= nu:
                o = (z + n_z - t) % n_z
                au_copy(t, o).wait_recv()
                if t < nu:
                    au_copy(t + 1, o).start()
                as_copy(o).start()
            o = (z + t) % n_z
            ad_copy(t, o).wait_recv()
            if t < nd:
                ad_copy(t + 1, o).start()
            as_copy(o).start()

    @pl.loop(1, n_z)
    def _(j):
        o = (z + j) % n_z
        mg_copy(o, o).wait_recv()

    units = float(LANES * 2 * n_z)
    for o in range(n_z):
        gn_out[:, o * LANES : (o + 1) * LANES] = sm_fin[o, :, :LANES] / units
        un_out[:, o * LANES : (o + 1) * LANES] = sm_fin[o, :, LANES : 2 * LANES] / units
    dn_out[...] = lax.dot_general(
        jnp.ones((8, LANES), F32), dnacc[...], CONTRACT_LAST,
        precision=lax.Precision.HIGHEST, preferred_element_type=F32,
    )[0:1, :] / float(LANES * n_z)
    for h in range(score_rows):
        at = slice(h * LANES, (h + 1) * LANES)
        gp = gp_ref[:, at]
        total = jnp.zeros((1, LANES), F32)
        for k in range(2):
            ep = ep_ref[k : k + 1, at]
            score = sm_fin[k * score_rows + h, :, 2 * LANES :] / (gp * ep)
            epg_out[k : k + 1, at] = gp * score
            total += ep * score
        gpg_out[:, at] = total

    @pl.when(c != ce)
    def _():
        @pl.loop(0, n_z)
        def _(o):
            as_copy(o).wait_recv()

    tg_store = pltpu.make_async_copy(tg, tg_out, out_sem.at[3])
    tg_store.start()

    for copy in grad_stores():
        copy.wait()

    @pl.loop(1, n_ep)
    def _(j):
        p = plane_peer(e, j, n_ep)
        in_copy(p, p, e).wait_send()
        sc_copy(p, e).wait_send()

    @pl.loop(0, n_ep)
    def _(s):
        za_copy(s, mine).wait_send()
        zb_copy(s, mine).wait_send()
        dx_copy(s, c).wait_send()
        dy_copy(s, c).wait_send()

    @pl.loop(0, n_z)
    def _(o):
        pt_copy(o).wait_send()

    @pl.loop(1, n_z)
    def _(j):
        o = (z + j) % n_z
        ms_copy(o, z).wait_send()
        mg_copy(z, o).wait_send()

    mx_copy().wait_send()
    for h in range(2):
        for t in range(nd):
            rd_copy(t, h).wait_send()
        for t in range(nu):
            ru_copy(t, h).wait_send()

    for i in range(per_core):
        b = c * per_core + i

        @pl.when(b != e)
        def _():
            fa_copy(i, b, e).wait_send()

    @pl.when(c == ce)
    def _():
        for t in range(1, nu + 1):
            au_copy(t, z).wait_send()
        for t in range(1, nd + 1):
            ad_copy(t, z).wait_send()

        @pl.loop(0, n_z)
        def _(o):
            as_copy(o).wait_send()

    tg_store.wait()


def local(tokens, cotangent, group_prob, expert_prob, routing, gate_weight, up_weight, down_weight):
    tok, width = tokens.shape
    n_ep = lax.axis_size("ep")
    n_z = lax.axis_size("tp") // 2
    cap = 3 * tok * 2 // (2 * n_ep)
    slots = n_ep * cap
    half = slots // 2
    quarter = width // 4
    unit = gate_weight.shape[2]
    nd, nu = n_z // 2, n_z // 2 - 1
    scw = -(-cap // LANES) * LANES
    dma = pltpu.SemaphoreType.DMA
    vm = pltpu.VMEM
    any_spec = pl.BlockSpec(memory_space=pl.ANY)
    vm_spec = pl.BlockSpec(memory_space=pltpu.VMEM)
    outs = pl.pallas_call(
        functools.partial(body, n_ep, n_z, cap),
        out_shape=(
            jax.ShapeDtypeStruct((tok, width), BF16),
            jax.ShapeDtypeStruct((1, width, unit), BF16),
            jax.ShapeDtypeStruct((1, width, unit), BF16),
            jax.ShapeDtypeStruct((1, unit, width), BF16),
            jax.ShapeDtypeStruct((1, width), F32),
            jax.ShapeDtypeStruct((1, width), F32),
            jax.ShapeDtypeStruct((1, unit), F32),
            jax.ShapeDtypeStruct((2, tok), F32),
            jax.ShapeDtypeStruct((1, tok), F32),
        ),
        in_specs=[vm_spec] * 3 + [any_spec] * 5,
        out_specs=(any_spec,) * 4 + (vm_spec,) * 5,
        scratch_shapes=[
            vm((tok, 2 * quarter), BF16),
            vm((2, slots, quarter), BF16),
            vm((2, 4, slots, quarter), BF16),
            vm((4, quarter, 2 * unit), BF16),
            vm((4, unit, quarter), BF16),
            vm((slots, 2 * unit), F32),
            vm((slots, unit), F32),
            vm((slots, 2 * unit), BF16),
            vm((2 * unit, slots), BF16),
            vm((unit, slots), BF16),
            vm((slots, unit), F32),
            vm((n_z, half, LANES), F32),
            vm((n_z, half, LANES), BF16),
            vm((n_z, half, LANES), BF16),
            vm((nd, half, LANES), BF16),
            vm((nd, half, LANES), BF16),
            vm((nu, half, LANES), BF16),
            vm((nu, half, LANES), BF16),
            vm((n_ep, 1, scw), F32),
            vm((n_ep, 1, scw), F32),
            vm((n_z, 1, 3 * LANES), F32),
            vm((n_z, 1, 3 * LANES), F32),
            vm((1, 3 * LANES), F32),
            vm((1, 3 * LANES), F32),
            vm((n_z, 1, 3 * LANES), F32),
            vm((half, LANES), BF16),
            vm((slots, LANES), BF16),
            vm((tok, width), BF16),
            vm((width, unit), BF16),
            vm((width, unit), BF16),
            vm((unit, width), BF16),
            vm((unit, LANES), F32),
            dma, dma((4, 3)), dma((2,)),
            dma((n_ep,)), dma((n_ep,)), dma((n_ep,)), dma((n_ep,)), dma((n_ep,)), dma((n_ep,)),
            dma((n_ep,)), dma((n_ep,)), dma((n_ep,)), dma((n_ep,)),
            dma((n_ep,)), dma((n_ep,)),
            dma((n_z,)), dma((n_z,)),
            dma((nd, 2)), dma((nd, 2)), dma((nu, 2)), dma((nu, 2)),
            dma((n_z,)), dma((n_z,)), dma((1,)), dma((1,)), dma((n_z,)), dma((n_z,)),
            dma((n_ep // 2,)), dma((n_ep,)),
            dma((nu + 1,)), dma((nu + 1,)), dma((nd + 1,)), dma((nd + 1,)),
            dma((n_z,)), dma((n_z,)),
            dma((4,)),
        ],
        compiler_params=pltpu.CompilerParams(
            collective_id=0, has_side_effects=True, vmem_limit_bytes=56 * 1024 * 1024
        ),
    )(
        routing.T, group_prob[None, :], expert_prob.T, tokens, cotangent,
        gate_weight, up_weight, down_weight,
    )
    tg, gg, ug, dg, gn, un, dn, epg, gpg = outs
    return tg, gpg[0], epg.T, gg, ug, dg, gn, un, dn


def solution(mesh):
    return jax.shard_map(
        local,
        mesh=mesh,
        in_specs=(
            P("ep", None),
            P("ep", None),
            P("ep"),
            P("ep", None),
            P("ep", None),
            P("ep", None, "tp"),
            P("ep", None, "tp"),
            P("ep", "tp", None),
        ),
        out_specs=(
            P("ep", None),
            P("ep"),
            P("ep", None),
            P("ep", None, "tp"),
            P("ep", None, "tp"),
            P("ep", "tp", None),
            P("ep", None),
            P("ep", None),
            P("ep", "tp"),
        ),
        check_vma=False,
    )
```

time: 326 us -> 134 us (0.41)
  the two profiles are of different devices: /device:TPU:96 before, /device:TPU:1 now
where the time goes in v1:
time: 134 us; the launch traced here: 133 us
  Pallas kernels  124 us (93%)
  local copies, waits for them, and re-layouts  8.69 us (6%)
    pallas_call x1, Pallas kernels, local(): pl.pallas_call(functools.partial(body, n_ep, n_z, cap), out_shape=(jax.Sh...  124 us
    unnamed x25, local copies, waits for them, and re-layouts  8.69 us

profile of v1, /device:TPU:1, one launch (start us, length us, event | category | flops | bytes accessed | tf_op | source)
XLA Modules:
  0.0 133.4 jit_solution(1571614650153167980)
XLA Ops:
  0.6 124.0 %shard_map.151 = (bf16[256,2048]{1,0:T(8,128)(2,1)}, bf16[1,2048,128]{2,1,0:T(8,128)(2,1)}, bf16[1,2048,128]{2,1,0:T(8,128)(2,1)}, bf16[1,128,2048]{2,1,0:T(8,12...) custom-call(s32[2,256]{1,0:T(2,128)} %bitcast.5, ...), custom_call_target="tpu_custom_call" | custom-call | tf_op jit(solution)/shard_map/pallas_call | solution.py:583
  124.7 0.0 copy-start.6
  124.7 0.0 copy-start.2
  124.7 2.4 %copy.26 = bf16[256,2048]{1,0:T(8,128)(2,1)} copy(bf16[256,2048]{1,0:T(8,128)(2,1)} %get-tuple-element.36) | data formatting | bytes 2097152
  127.1 0.0 copy-done.6
  127.1 0.0 copy-start.5
  127.1 0.6 copy.27
  127.6 0.1 copy-done.5
  127.7 0.6 copy.28
  128.3 0.0 copy-done.2
  128.3 0.0 copy-start.1
  128.3 0.8 copy.29
  129.1 0.4 copy-done.1
  129.5 0.0 copy-start
  129.5 0.8 copy.30
  130.3 0.4 copy-done
  130.8 0.0 copy-start.4
  130.8 0.8 copy.31
  131.6 0.0 copy-done.4
  131.6 0.0 copy-start.3
  131.6 0.6 copy.32
  132.2 0.1 copy-done.3
  132.3 0.0 copy-start.7
  132.3 0.6 copy.33
  132.9 0.0 copy-done.7
  132.9 0.5 copy.34
Async XLA Ops:
  124.7 2.4 %copy-start.6 = (f32[1,256]{1,0:T(1,128)S(1)}, f32[1,256]{1,0:T(1,128)}, u32[]{:S(2)}) copy-start(f32[1,256]{1,0:T(1,128)} %get-tuple-element.19) | copy-start | bytes 3076
  124.7 3.6 %copy-start.2 = (bf16[1,2048,128]{2,1,0:T(8,128)(2,1)S(1)}, bf16[1,2048,128]{2,1,0:T(8,128)(2,1)}, u32[]{:S(2)}) copy-start(bf16[1,2048,128]{2,1,0:T(8,128)(2,1)} %get-tuple-element.39) | copy-start | bytes 1572868
  127.1 0.7 copy-start.5
  128.3 1.2 copy-start.1
  129.5 1.2 copy-start
  130.8 0.8 copy-start.4
  131.6 0.7 copy-start.3
  132.3 0.6 copy-start.7

commit v2 on v1

--- a/solution.py
+++ b/solution.py
@@ -11,6 +11,9 @@
 F32 = jnp.float32
 BF16 = jnp.bfloat16
 CONTRACT_LAST = (((1,), (1,)), ((), ()))
+SUM_PIECES = 4
+GATHER_PIECES = 2
+GATHER_CORE = 1
 
 
 def plane_peer(e, j, n_ep):
@@ -57,7 +60,7 @@
     fin, gat, tg, gg, ug, dg, dnacc,
     ld_sem, wl_sem, loc_sem, in_s, in_r, za_s, za_r, zb_s, zb_r, dx_s, dx_r, dy_s, dy_r,
     sc_s, sc_r, pt_s, pt_r, rd_s, rd_r, ru_s, ru_r, ms_s, ms_r, mx_s, mx_r, mg_s, mg_r,
-    fa_s, fa_r, au_s, au_r, ad_s, ad_r, as_s, as_r, out_sem,
+    fa_s, fa_r, au_s, au_r, ad_s, ad_r, as_s, as_r, out_sem, met4, met8, pickt,
 ):
     e, tp = lax.axis_index("ep"), lax.axis_index("tp")
     z, c = tp // 2, tp % 2
@@ -89,11 +92,14 @@
             barrier, inc=1, device_id=(plane_peer(e, j, n_ep), tp), device_id_type=MESH
         )
 
-    @pl.loop(1, n_z)
-    def _(j):
-        pl.semaphore_signal(barrier, inc=1, device_id=at_z((z + j) % n_z), device_id_type=MESH)
-
+    for step in (1, 2):
+        for o in (z + step, z + n_z - step):
+            pl.semaphore_signal(barrier, inc=1, device_id=at_z(o % n_z), device_id_type=MESH)
     pl.semaphore_signal(barrier, inc=1, device_id=sibling, device_id_type=MESH)
+
+    def greet(sem, step):
+        for o in (z + step, z + n_z - step):
+            pl.semaphore_signal(sem, inc=1, device_id=at_z(o % n_z), device_id_type=MESH)
 
     start_col = pl.multiple_of(par * (2 * quarter), LANES)
 
@@ -137,7 +143,8 @@
         send[0, pl.ds(at, LANES), :] = got[:, :quarter].astype(BF16)
         send[1, pl.ds(at, LANES), :] = got[:, quarter:].astype(BF16)
 
-    pl.semaphore_wait(barrier, n_ep - 1 + n_z - 1 + 1)
+    pl.semaphore_wait(barrier, n_ep - 1 + 4 + 1)
+    greet(met4, 2)
 
     def block(b):
         return pl.ds(pl.multiple_of(b * cap, 16), cap)
@@ -189,6 +196,9 @@
         zb_copy(s, mine).start()
         dx_copy(s, c).start()
 
+    pl.semaphore_wait(met4, 2)
+    greet(met8, 4)
+
     @pl.loop(0, n_ep)
     def _(j):
         s = plane_source(e, j, n_ep)
@@ -204,6 +214,8 @@
         s = plane_source(e, j, n_ep)
         dx_copy(s, 1 - c).wait_recv()
         dy_copy(s, 1 - c).wait_recv()
+
+    pl.semaphore_wait(met8, 2)
 
     pre[...] = jnp.zeros_like(pre)
     hg[...] = jnp.zeros_like(hg)
@@ -265,19 +277,24 @@
 
     dnacc[...] = jnp.zeros_like(dnacc)
 
-    def weight_quarter(q):
+    def down_piece(q):
         down = jnp.dot(hidt[...], rows[1, q], preferred_element_type=F32)
         dg[:, q * quarter : (q + 1) * quarter] = down.astype(BF16)
         square = down * down
         dnacc[...] += sum(square[:, i * LANES : (i + 1) * LANES] for i in range(qc))
-        for k, target in enumerate((gg, ug)):
-            both = jnp.dot(
-                gput[k * LANES : (k + 1) * LANES, :], rows[0, q], preferred_element_type=F32
-            )
-            norm = jnp.sum(both * both, axis=0, keepdims=True)
-            for i in range(qc):
-                sm[q * qc + i, :, k * LANES : (k + 1) * LANES] = norm[:, i * LANES : (i + 1) * LANES]
-            target[q * quarter : (q + 1) * quarter, :] = both.T.astype(BF16)
+
+    def in_piece(k, q):
+        target = (gg, ug)[k]
+        both = jnp.dot(gput[k * LANES : (k + 1) * LANES, :], rows[0, q], preferred_element_type=F32)
+        norm = jnp.sum(both * both, axis=0, keepdims=True)
+        for i in range(qc):
+            sm[q * qc + i, :, k * LANES : (k + 1) * LANES] = norm[:, i * LANES : (i + 1) * LANES]
+        target[q * quarter : (q + 1) * quarter, :] = both.T.astype(BF16)
+
+    def pick_piece():
+        lane = lax.broadcasted_iota(jnp.int32, (slots, tok), 0).astype(F32)
+        pick = jnp.where((lane == slot0) | (lane == slot1), 1.0, 0.0)
+        pickt[...] = pick.T.astype(BF16)
 
     def grad_stores():
         return [
@@ -346,7 +363,17 @@
         def _(j):
             mg_copy(z, (z + j) % n_z).start()
 
-    sub = half // 2
+    def store_start():
+        for copy in grad_stores():
+            copy.start()
+
+    work = []
+    for q in range(4):
+        work += [functools.partial(down_piece, q)]
+        work += [functools.partial(in_piece, 0, q), functools.partial(in_piece, 1, q)]
+    work += [small_start, store_start, pick_piece]
+
+    sub = half // SUM_PIECES
 
     def part(h):
         return pl.ds(h * sub, sub)
@@ -370,7 +397,7 @@
         o_dn, o_up = (z + n_z - nd + t) % n_z, (z + nu - t + n_z) % n_z
         pt_copy(o_dn).wait_recv()
         pt_copy(o_up).wait_recv()
-        for h in range(2):
+        for h in range(SUM_PIECES):
             total = chip_sum(o_dn, h)
             if t > 0:
                 rd_copy(t - 1, h).wait_recv()
@@ -384,24 +411,14 @@
                     total += up_recv[t - 1, part(h), :].astype(F32)
                 up_send[t, part(h), :] = total.astype(BF16)
                 ru_copy(t, h).start()
-        if n_z == 16:
-            if t < 4:
-                weight_quarter(t)
-            if t == 3:
-                small_start()
-                for copy in grad_stores():
-                    copy.start()
-            if t == 6:
-                small_middle()
-        elif t == 0:
-            for q in range(4):
-                weight_quarter(q)
-            small_start()
-            for copy in grad_stores():
-                copy.start()
+            for _ in range(1 if n_z == 16 else len(work)):
+                if work:
+                    work.pop(0)()
+        if t == nd - 2:
             small_middle()
 
-    for h in range(2):
+    small_end()
+    for h in range(SUM_PIECES):
         total = chip_sum(z, h)
         ru_copy(nu - 1, h).wait_recv()
         total += up_recv[nu - 1, part(h), :].astype(F32)
@@ -410,13 +427,16 @@
         fin[part(h), :] = total.astype(BF16)
 
     per_core = n_ep // 2
-    ce = e // per_core
+    own_core = e // per_core
 
     def fa_copy(i, to, sender):
         return remote(
             fin.at[pl.ds(i * cap, cap), :], gat.at[block(sender), :],
-            fa_s.at[i], fa_r.at[sender], (to, tp),
-        )
+            fa_s.at[i], fa_r.at[sender], (to, z * 2 + GATHER_CORE),
+        )
+
+    def stays(b):
+        return (b == e) & (c == GATHER_CORE)
 
     def fa_local(i):
         return pltpu.make_async_copy(
@@ -426,57 +446,66 @@
     for i in range(per_core):
         b = c * per_core + i
 
-        @pl.when(b != e)
+        @pl.when(jnp.logical_not(stays(b)))
         def _():
             fa_copy(i, b, e).start()
 
-        @pl.when(b == e)
+        @pl.when(stays(b))
         def _():
             fa_local(i).start()
 
-    small_end()
-
-    def chunk(o):
-        return tg.at[:, pl.ds(pl.multiple_of(o * LANES, LANES), LANES)]
-
-    def au_copy(t, o):
-        return remote(chunk(o), chunk(o), au_s.at[t], au_r.at[t], at_z(up_z))
-
-    def ad_copy(t, o):
-        return remote(chunk(o), chunk(o), ad_s.at[t], ad_r.at[t], at_z(dn_z))
-
-    def as_copy(o):
-        return remote(chunk(o), chunk(o), as_s.at[o], as_r.at[o], sibling)
-
-    @pl.when(c == ce)
+    piece = tok // GATHER_PIECES
+
+    def chunk(o, h):
+        return tg.at[pl.ds(h * piece, piece), pl.ds(pl.multiple_of(o * LANES, LANES), LANES)]
+
+    def au_copy(t, h, o):
+        ref = chunk(o, h)
+        return remote(ref, ref, au_s.at[t, h], au_r.at[t, h], at_z(up_z))
+
+    def ad_copy(t, h, o):
+        ref = chunk(o, h)
+        return remote(ref, ref, ad_s.at[t, h], ad_r.at[t, h], at_z(dn_z))
+
+    def as_copy(o, h):
+        ref = chunk(o, h)
+        return remote(ref, ref, as_s.at[o, h], as_r.at[o, h], sibling)
+
+    @pl.when(c == GATHER_CORE)
     def _():
-        fa_local(0).wait()
+        @pl.when(own_core == GATHER_CORE)
+        def _():
+            fa_local(0).wait()
+
+        @pl.when(own_core != GATHER_CORE)
+        def _():
+            fa_copy(0, e, e).wait_recv()
 
         @pl.loop(1, n_ep)
         def _(j):
             s = (e + j) % n_ep
             fa_copy(0, s, s).wait_recv()
 
-        acc = jnp.zeros((tok, LANES), F32)
-        lane = lax.broadcasted_iota(jnp.int32, (slots, tok), 0).astype(F32)
-        pick = jnp.where((lane == slot0) | (lane == slot1), 1.0, 0.0)
-        acc = jnp.dot(pick.T.astype(BF16), gat[...], preferred_element_type=F32)
-        tg[:, pl.ds(pl.multiple_of(z * LANES, LANES), LANES)] = acc.astype(BF16)
-        au_copy(1, z).start()
-        ad_copy(1, z).start()
-        as_copy(z).start()
+        for h in range(GATHER_PIECES):
+            at = slice(h * piece, (h + 1) * piece)
+            acc = jnp.dot(pickt[at, :], gat[...], preferred_element_type=F32)
+            tg[at, pl.ds(pl.multiple_of(z * LANES, LANES), LANES)] = acc.astype(BF16)
+            au_copy(1, h, z).start()
+            ad_copy(1, h, z).start()
+            as_copy(z, h).start()
         for t in range(1, nd + 1):
-            if t <= nu:
-                o = (z + n_z - t) % n_z
-                au_copy(t, o).wait_recv()
-                if t < nu:
-                    au_copy(t + 1, o).start()
-                as_copy(o).start()
-            o = (z + t) % n_z
-            ad_copy(t, o).wait_recv()
-            if t < nd:
-                ad_copy(t + 1, o).start()
-            as_copy(o).start()
+            for h in range(GATHER_PIECES):
+                if t <= nu:
+                    o = (z + n_z - t) % n_z
+                    au_copy(t, h, o).wait_recv()
+                    if t < nu:
+                        au_copy(t + 1, h, o).start()
+                    as_copy(o, h).start()
+                o = (z + t) % n_z
+                ad_copy(t, h, o).wait_recv()
+                if t < nd:
+                    ad_copy(t + 1, h, o).start()
+                as_copy(o, h).start()
 
     @pl.loop(1, n_z)
     def _(j):
@@ -502,11 +531,12 @@
             total += ep * score
         gpg_out[:, at] = total
 
-    @pl.when(c != ce)
+    @pl.when(c != GATHER_CORE)
     def _():
         @pl.loop(0, n_z)
         def _(o):
-            as_copy(o).wait_recv()
+            for h in range(GATHER_PIECES):
+                as_copy(o, h).wait_recv()
 
     tg_store = pltpu.make_async_copy(tg, tg_out, out_sem.at[3])
     tg_store.start()
@@ -538,7 +568,7 @@
         mg_copy(z, o).wait_send()
 
     mx_copy().wait_send()
-    for h in range(2):
+    for h in range(SUM_PIECES):
         for t in range(nd):
             rd_copy(t, h).wait_send()
         for t in range(nu):
@@ -547,22 +577,50 @@
     for i in range(per_core):
         b = c * per_core + i
 
-        @pl.when(b != e)
+        @pl.when(jnp.logical_not(stays(b)))
         def _():
             fa_copy(i, b, e).wait_send()
 
-    @pl.when(c == ce)
+    @pl.when(c == GATHER_CORE)
     def _():
-        for t in range(1, nu + 1):
-            au_copy(t, z).wait_send()
-        for t in range(1, nd + 1):
-            ad_copy(t, z).wait_send()
-
-        @pl.loop(0, n_z)
-        def _(o):
-            as_copy(o).wait_send()
+        for h in range(GATHER_PIECES):
+            for t in range(1, nu + 1):
+                au_copy(t, h, z).wait_send()
+            for t in range(1, nd + 1):
+                ad_copy(t, h, z).wait_send()
+
+            @pl.loop(0, n_z)
+            def _(o):
+                as_copy(o, h).wait_send()
 
     tg_store.wait()
+
+
+def flush(count, *refs):
+    ins, outs, bufs = refs[:count], refs[count : 2 * count], refs[2 * count : 3 * count]
+    in_sem, out_sem = refs[3 * count :]
+    reads = [pltpu.make_async_copy(ins[i], bufs[i], in_sem.at[i]) for i in range(count)]
+    writes = [pltpu.make_async_copy(bufs[i], outs[i], out_sem.at[i]) for i in range(count)]
+    for copy in reads:
+        copy.start()
+    for i in range(count):
+        reads[i].wait()
+        writes[i].start()
+    for copy in writes:
+        copy.wait()
+
+
+def write_out(arrays):
+    count = len(arrays)
+    any_spec = pl.BlockSpec(memory_space=pl.ANY)
+    return pl.pallas_call(
+        functools.partial(flush, count),
+        out_shape=tuple(jax.ShapeDtypeStruct(a.shape, a.dtype) for a in arrays),
+        in_specs=[any_spec] * count,
+        out_specs=(any_spec,) * count,
+        scratch_shapes=[pltpu.VMEM(a.shape, a.dtype) for a in arrays]
+        + [pltpu.SemaphoreType.DMA((count,)), pltpu.SemaphoreType.DMA((count,))],
+    )(*arrays)
 
 
 def local(tokens, cotangent, group_prob, expert_prob, routing, gate_weight, up_weight, down_weight):
@@ -633,12 +691,14 @@
             dma((n_ep,)), dma((n_ep,)), dma((n_ep,)), dma((n_ep,)),
             dma((n_ep,)), dma((n_ep,)),
             dma((n_z,)), dma((n_z,)),
-            dma((nd, 2)), dma((nd, 2)), dma((nu, 2)), dma((nu, 2)),
+            dma((nd, SUM_PIECES)), dma((nd, SUM_PIECES)), dma((nu, SUM_PIECES)), dma((nu, SUM_PIECES)),
             dma((n_z,)), dma((n_z,)), dma((1,)), dma((1,)), dma((n_z,)), dma((n_z,)),
             dma((n_ep // 2,)), dma((n_ep,)),
-            dma((nu + 1,)), dma((nu + 1,)), dma((nd + 1,)), dma((nd + 1,)),
-            dma((n_z,)), dma((n_z,)),
-            dma((4,)),
+            dma((nu + 1, GATHER_PIECES)), dma((nu + 1, GATHER_PIECES)),
+            dma((nd + 1, GATHER_PIECES)), dma((nd + 1, GATHER_PIECES)),
+            dma((n_z, GATHER_PIECES)), dma((n_z, GATHER_PIECES)),
+            dma((4,)), pltpu.SemaphoreType.REGULAR, pltpu.SemaphoreType.REGULAR,
+            vm((tok, slots), BF16),
         ],
         compiler_params=pltpu.CompilerParams(
             collective_id=0, has_side_effects=True, vmem_limit_bytes=56 * 1024 * 1024
@@ -647,7 +707,7 @@
         routing.T, group_prob[None, :], expert_prob.T, tokens, cotangent,
         gate_weight, up_weight, down_weight,
     )
-    tg, gg, ug, dg, gn, un, dn, epg, gpg = outs
+    tg, gg, ug, dg, gn, un, dn, epg, gpg = write_out(outs)
     return tg, gpg[0], epg.T, gg, ug, dg, gn, un, dn
 
 

time: 134 us -> 115 us (0.86)
  Pallas kernels: 124 us -> 114 us
  local copies, waits for them, and re-layouts: 8.69 us -> 0 us
    pallas_call x1, Pallas kernels: 124 us -> 112 us  [local(): pl.pallas_call(functools.partial(body, n_ep, n_z, cap), out_shape=(jax.Sh...]
    unnamed x25 -> x0, local copies, waits for them, and re-layouts: 8.69 us -> none
    pallas_call x0 -> x1, Pallas kernels: none -> 2.88 us  [write_out(): pl.pallas_call(functools.partial(flush, count), out_shape=tuple((jax.Shap...]
where the time goes in v2:
time: 115 us
  Pallas kernels  114 us (99%)
    pallas_call x1, Pallas kernels, local(): pl.pallas_call(functools.partial(body, n_ep, n_z, cap), out_shape=(jax.Sh...  112 us
    pallas_call x1, Pallas kernels, write_out(): pl.pallas_call(functools.partial(flush, count), out_shape=tuple((jax.Shap...  2.88 us

profile of v2, /device:TPU:1, one launch (start us, length us, event | category | flops | bytes accessed | tf_op | source)
XLA Modules:
  0.0 115.1 jit_solution(16632160104614562958)
XLA Ops:
  0.6 111.5 %shard_map.151 = (bf16[256,2048]{1,0:T(8,128)(2,1)}, bf16[1,2048,128]{2,1,0:T(8,128)(2,1)}, bf16[1,2048,128]{2,1,0:T(8,128)(2,1)}, bf16[1,128,2048]{2,1,0:T(8,12...) custom-call(s32[2,256]{1,0:T(2,128)} %bitcast.5, ...), custom_call_target="tpu_custom_call" | custom-call | tf_op jit(solution)/shard_map/pallas_call | solution.py:641
  112.2 2.9 %shard_map.152 = (bf16[256,2048]{1,0:T(8,128)(2,1)}, bf16[1,2048,128]{2,1,0:T(8,128)(2,1)}, bf16[1,2048,128]{2,1,0:T(8,128)(2,1)}, bf16[1,128,2048]{2,1,0:T(8,12...) custom-call(bf16[256,2048]{1,0:T(8,128)(2,1)} %get-tuple-element.27., ...), custom_call_target="tpu_custom_call" | custom-call | tf_op jit(solution)/shard_map/pallas_call | solution.py:616

commit v3 on v2

--- a/solution.py
+++ b/solution.py
@@ -13,7 +13,7 @@
 CONTRACT_LAST = (((1,), (1,)), ((), ()))
 SUM_PIECES = 4
 GATHER_PIECES = 2
-GATHER_CORE = 1
+CHAIN_CORE = 1
 
 
 def plane_peer(e, j, n_ep):
@@ -70,7 +70,6 @@
     up_z, dn_z = (z + 1) % n_z, (z + n_z - 1) % n_z
     tok, quarter = x.shape[0], rows.shape[3]
     slots = n_ep * cap
-    half = slots // 2
     nd, nu = n_z // 2, n_z // 2 - 1
     qc = quarter // LANES
     sibling = (e, z * 2 + 1 - c)
@@ -143,6 +142,8 @@
         send[0, pl.ds(at, LANES), :] = got[:, :quarter].astype(BF16)
         send[1, pl.ds(at, LANES), :] = got[:, quarter:].astype(BF16)
 
+    pre[...] = jnp.zeros_like(pre)
+    hg[...] = jnp.zeros_like(hg)
     pl.semaphore_wait(barrier, n_ep - 1 + 4 + 1)
     greet(met4, 2)
 
@@ -196,8 +197,32 @@
         zb_copy(s, mine).start()
         dx_copy(s, c).start()
 
+    def gate_up_part(q):
+        pre[...] += jnp.dot(rows[0, q], wgu[q], preferred_element_type=F32)
+
+    def down_part(q):
+        hg[...] += lax.dot_general(rows[1, q], wd[q], CONTRACT_LAST, preferred_element_type=F32)
+
+    def multiply(first, arr_is_own):
+        is_in = (c == 0) if arr_is_own else (c == 1)
+
+        @pl.when(is_in)
+        def _():
+            @pl.loop(0, 2)
+            def _(i):
+                gate_up_part(first + i)
+
+        @pl.when(jnp.logical_not(is_in))
+        def _():
+            @pl.loop(0, 2)
+            def _(i):
+                down_part(first + i)
+
+    for copy in weight_loads():
+        copy.wait()
     pl.semaphore_wait(met4, 2)
     greet(met8, 4)
+    multiply(mine, True)
 
     @pl.loop(0, n_ep)
     def _(j):
@@ -206,24 +231,20 @@
         zb_copy(s, other).wait_recv()
         dy_copy(s, c).start()
 
-    for copy in weight_loads():
-        copy.wait()
+    multiply(other, True)
 
     @pl.loop(0, n_ep)
     def _(j):
-        s = plane_source(e, j, n_ep)
-        dx_copy(s, 1 - c).wait_recv()
-        dy_copy(s, 1 - c).wait_recv()
+        dx_copy(plane_source(e, j, n_ep), 1 - c).wait_recv()
+
+    multiply(mine, False)
+
+    @pl.loop(0, n_ep)
+    def _(j):
+        dy_copy(plane_source(e, j, n_ep), 1 - c).wait_recv()
 
     pl.semaphore_wait(met8, 2)
-
-    pre[...] = jnp.zeros_like(pre)
-    hg[...] = jnp.zeros_like(hg)
-
-    @pl.loop(0, 4)
-    def _(q):
-        pre[...] += jnp.dot(rows[0, q], wgu[q], preferred_element_type=F32)
-        hg[...] += lax.dot_general(rows[1, q], wd[q], CONTRACT_LAST, preferred_element_type=F32)
+    multiply(other, False)
 
     @pl.loop(0, slots // LANES)
     def _(i):
@@ -242,38 +263,32 @@
         gput[LANES:, at] = up_pre.T.astype(BF16)
         hidt[:, at] = hidden.T.astype(BF16)
 
-    ones = jnp.ones((8, LANES), F32)
-    for b in range(n_ep):
-        row = lax.dot_general(
-            ones, prod[b * cap : (b + 1) * cap, :], CONTRACT_LAST,
-            precision=lax.Precision.HIGHEST, preferred_element_type=F32,
-        )
-        sc_send[b, :, :cap] = row[0:1, :]
-
     def sc_copy(to, sender):
         return remote(sc_send.at[to], sc_recv.at[sender], sc_s.at[to], sc_r.at[sender], (to, tp))
 
-    @pl.loop(1, n_ep)
-    def _(j):
-        p = plane_peer(e, j, n_ep)
-        sc_copy(p, e).start()
-
-    keep = pl.ds(pl.multiple_of(c * half, 16), half)
-    give = pl.ds(pl.multiple_of((1 - c) * half, 16), half)
-
     def pt_copy(o):
         return remote(sib_send.at[o], sib_recv.at[o], pt_s.at[o], pt_r.at[o], sibling)
 
-    @pl.loop(0, 4)
-    def _(q):
-        given = lax.dot_general(gpu[give, :], wgu[q], CONTRACT_LAST, preferred_element_type=F32)
-        for i in range(qc):
-            sib_send[q * qc + i] = given[:, i * LANES : (i + 1) * LANES].astype(BF16)
-        for i in range(qc):
-            pt_copy(q * qc + i).start()
-        kept = lax.dot_general(gpu[keep, :], wgu[q], CONTRACT_LAST, preferred_element_type=F32)
-        for i in range(qc):
-            own[q * qc + i] = kept[:, i * LANES : (i + 1) * LANES]
+    def input_part(q):
+        return lax.dot_general(gpu[...], wgu[q], CONTRACT_LAST, preferred_element_type=F32)
+
+    def quarters():
+        return [((z + nd) // qc + step) % 4 for step in (0, 3, 1, 2)]
+
+    @pl.when(c != CHAIN_CORE)
+    def _():
+        for q in quarters():
+            part = input_part(q)
+            for i in range(qc):
+                sib_send[q * qc + i] = part[:, i * LANES : (i + 1) * LANES].astype(BF16)
+                pt_copy(q * qc + i).start()
+
+    @pl.when(c == CHAIN_CORE)
+    def _():
+        for q in quarters():
+            part = input_part(q)
+            for i in range(qc):
+                own[q * qc + i] = part[:, i * LANES : (i + 1) * LANES]
 
     dnacc[...] = jnp.zeros_like(dnacc)
 
@@ -363,17 +378,31 @@
         def _(j):
             mg_copy(z, (z + j) % n_z).start()
 
+    def scores():
+        ones = jnp.ones((8, LANES), F32)
+        for b in range(n_ep):
+            row = lax.dot_general(
+                ones, prod[b * cap : (b + 1) * cap, :], CONTRACT_LAST,
+                precision=lax.Precision.HIGHEST, preferred_element_type=F32,
+            )
+            sc_send[b, :, :cap] = row[0:1, :]
+
+        @pl.loop(1, n_ep)
+        def _(j):
+            p = plane_peer(e, j, n_ep)
+            sc_copy(p, e).start()
+
     def store_start():
         for copy in grad_stores():
             copy.start()
 
-    work = []
+    work = [scores]
     for q in range(4):
         work += [functools.partial(down_piece, q)]
         work += [functools.partial(in_piece, 0, q), functools.partial(in_piece, 1, q)]
-    work += [small_start, store_start, pick_piece]
-
-    sub = half // SUM_PIECES
+    work += [small_start, store_start]
+
+    sub = slots // SUM_PIECES
 
     def part(h):
         return pl.ds(h * sub, sub)
@@ -393,66 +422,56 @@
     def chip_sum(o, h):
         return own[o, part(h), :] + sib_recv[o, part(h), :].astype(F32)
 
-    for t in range(nd):
-        o_dn, o_up = (z + n_z - nd + t) % n_z, (z + nu - t + n_z) % n_z
-        pt_copy(o_dn).wait_recv()
-        pt_copy(o_up).wait_recv()
+    @pl.when(c != CHAIN_CORE)
+    def _():
+        for step in work:
+            step()
+        small_middle()
+        small_end()
+
+    @pl.when(c == CHAIN_CORE)
+    def _():
+        todo = work + [pick_piece]
+        for t in range(nd):
+            o_dn, o_up = (z + n_z - nd + t) % n_z, (z + nu - t + n_z) % n_z
+            pt_copy(o_dn).wait_recv()
+            pt_copy(o_up).wait_recv()
+            for h in range(SUM_PIECES):
+                total = chip_sum(o_dn, h)
+                if t > 0:
+                    rd_copy(t - 1, h).wait_recv()
+                    total += dn_recv[t - 1, part(h), :].astype(F32)
+                dn_send[t, part(h), :] = total.astype(BF16)
+                rd_copy(t, h).start()
+                if t < nu:
+                    total = chip_sum(o_up, h)
+                    if t > 0:
+                        ru_copy(t - 1, h).wait_recv()
+                        total += up_recv[t - 1, part(h), :].astype(F32)
+                    up_send[t, part(h), :] = total.astype(BF16)
+                    ru_copy(t, h).start()
+                for _ in range(1 if n_z == 16 else len(todo)):
+                    if todo:
+                        todo.pop(0)()
+            if t == nd - 2:
+                small_middle()
+
+        small_end()
         for h in range(SUM_PIECES):
-            total = chip_sum(o_dn, h)
-            if t > 0:
-                rd_copy(t - 1, h).wait_recv()
-                total += dn_recv[t - 1, part(h), :].astype(F32)
-            dn_send[t, part(h), :] = total.astype(BF16)
-            rd_copy(t, h).start()
-            if t < nu:
-                total = chip_sum(o_up, h)
-                if t > 0:
-                    ru_copy(t - 1, h).wait_recv()
-                    total += up_recv[t - 1, part(h), :].astype(F32)
-                up_send[t, part(h), :] = total.astype(BF16)
-                ru_copy(t, h).start()
-            for _ in range(1 if n_z == 16 else len(work)):
-                if work:
-                    work.pop(0)()
-        if t == nd - 2:
-            small_middle()
-
-    small_end()
-    for h in range(SUM_PIECES):
-        total = chip_sum(z, h)
-        ru_copy(nu - 1, h).wait_recv()
-        total += up_recv[nu - 1, part(h), :].astype(F32)
-        rd_copy(nd - 1, h).wait_recv()
-        total += dn_recv[nd - 1, part(h), :].astype(F32)
-        fin[part(h), :] = total.astype(BF16)
-
-    per_core = n_ep // 2
-    own_core = e // per_core
-
-    def fa_copy(i, to, sender):
+            total = chip_sum(z, h)
+            ru_copy(nu - 1, h).wait_recv()
+            total += up_recv[nu - 1, part(h), :].astype(F32)
+            rd_copy(nd - 1, h).wait_recv()
+            total += dn_recv[nd - 1, part(h), :].astype(F32)
+            fin[part(h), :] = total.astype(BF16)
+
+    def fa_copy(b, sender):
         return remote(
-            fin.at[pl.ds(i * cap, cap), :], gat.at[block(sender), :],
-            fa_s.at[i], fa_r.at[sender], (to, z * 2 + GATHER_CORE),
+            fin.at[block(b), :], gat.at[block(sender), :], fa_s.at[b], fa_r.at[sender], (b, tp)
         )
 
-    def stays(b):
-        return (b == e) & (c == GATHER_CORE)
-
-    def fa_local(i):
-        return pltpu.make_async_copy(
-            fin.at[pl.ds(i * cap, cap), :], gat.at[block(e), :], loc_sem.at[1]
-        )
-
-    for i in range(per_core):
-        b = c * per_core + i
-
-        @pl.when(jnp.logical_not(stays(b)))
-        def _():
-            fa_copy(i, b, e).start()
-
-        @pl.when(stays(b))
-        def _():
-            fa_local(i).start()
+    def fa_local():
+        return pltpu.make_async_copy(fin.at[block(e), :], gat.at[block(e), :], loc_sem.at[1])
 
     piece = tok // GATHER_PIECES
 
@@ -471,20 +490,20 @@
         ref = chunk(o, h)
         return remote(ref, ref, as_s.at[o, h], as_r.at[o, h], sibling)
 
-    @pl.when(c == GATHER_CORE)
-    def _():
-        @pl.when(own_core == GATHER_CORE)
-        def _():
-            fa_local(0).wait()
-
-        @pl.when(own_core != GATHER_CORE)
-        def _():
-            fa_copy(0, e, e).wait_recv()
+    @pl.when(c == CHAIN_CORE)
+    def _():
+        fa_local().start()
 
         @pl.loop(1, n_ep)
         def _(j):
-            s = (e + j) % n_ep
-            fa_copy(0, s, s).wait_recv()
+            fa_copy(plane_peer(e, j, n_ep), e).start()
+
+        fa_local().wait()
+
+        @pl.loop(1, n_ep)
+        def _(j):
+            s = plane_source(e, j, n_ep)
+            fa_copy(s, s).wait_recv()
 
         for h in range(GATHER_PIECES):
             at = slice(h * piece, (h + 1) * piece)
@@ -531,7 +550,7 @@
             total += ep * score
         gpg_out[:, at] = total
 
-    @pl.when(c != GATHER_CORE)
+    @pl.when(c != CHAIN_CORE)
     def _():
         @pl.loop(0, n_z)
         def _(o):
@@ -557,10 +576,6 @@
         dx_copy(s, c).wait_send()
         dy_copy(s, c).wait_send()
 
-    @pl.loop(0, n_z)
-    def _(o):
-        pt_copy(o).wait_send()
-
     @pl.loop(1, n_z)
     def _(j):
         o = (z + j) % n_z
@@ -568,20 +583,25 @@
         mg_copy(z, o).wait_send()
 
     mx_copy().wait_send()
-    for h in range(SUM_PIECES):
-        for t in range(nd):
-            rd_copy(t, h).wait_send()
-        for t in range(nu):
-            ru_copy(t, h).wait_send()
-
-    for i in range(per_core):
-        b = c * per_core + i
-
-        @pl.when(jnp.logical_not(stays(b)))
-        def _():
-            fa_copy(i, b, e).wait_send()
-
-    @pl.when(c == GATHER_CORE)
+    @pl.when(c != CHAIN_CORE)
+    def _():
+        @pl.loop(0, n_z)
+        def _(o):
+            pt_copy(o).wait_send()
+
+    @pl.when(c == CHAIN_CORE)
+    def _():
+        @pl.loop(1, n_ep)
+        def _(j):
+            fa_copy(plane_peer(e, j, n_ep), e).wait_send()
+
+        for h in range(SUM_PIECES):
+            for t in range(nd):
+                rd_copy(t, h).wait_send()
+            for t in range(nu):
+                ru_copy(t, h).wait_send()
+
+    @pl.when(c == CHAIN_CORE)
     def _():
         for h in range(GATHER_PIECES):
             for t in range(1, nu + 1):
@@ -629,7 +649,6 @@
     n_z = lax.axis_size("tp") // 2
     cap = 3 * tok * 2 // (2 * n_ep)
     slots = n_ep * cap
-    half = slots // 2
     quarter = width // 4
     unit = gate_weight.shape[2]
     nd, nu = n_z // 2, n_z // 2 - 1
@@ -665,13 +684,13 @@
             vm((2 * unit, slots), BF16),
             vm((unit, slots), BF16),
             vm((slots, unit), F32),
-            vm((n_z, half, LANES), F32),
-            vm((n_z, half, LANES), BF16),
-            vm((n_z, half, LANES), BF16),
-            vm((nd, half, LANES), BF16),
-            vm((nd, half, LANES), BF16),
-            vm((nu, half, LANES), BF16),
-            vm((nu, half, LANES), BF16),
+            vm((n_z, slots, LANES), F32),
+            vm((n_z, slots, LANES), BF16),
+            vm((n_z, slots, LANES), BF16),
+            vm((nd, slots, LANES), BF16),
+            vm((nd, slots, LANES), BF16),
+            vm((nu, slots, LANES), BF16),
+            vm((nu, slots, LANES), BF16),
             vm((n_ep, 1, scw), F32),
             vm((n_ep, 1, scw), F32),
             vm((n_z, 1, 3 * LANES), F32),
@@ -679,7 +698,7 @@
             vm((1, 3 * LANES), F32),
             vm((1, 3 * LANES), F32),
             vm((n_z, 1, 3 * LANES), F32),
-            vm((half, LANES), BF16),
+            vm((slots, LANES), BF16),
             vm((slots, LANES), BF16),
             vm((tok, width), BF16),
             vm((width, unit), BF16),
@@ -693,7 +712,7 @@
             dma((n_z,)), dma((n_z,)),
             dma((nd, SUM_PIECES)), dma((nd, SUM_PIECES)), dma((nu, SUM_PIECES)), dma((nu, SUM_PIECES)),
             dma((n_z,)), dma((n_z,)), dma((1,)), dma((1,)), dma((n_z,)), dma((n_z,)),
-            dma((n_ep // 2,)), dma((n_ep,)),
+            dma((n_ep,)), dma((n_ep,)),
             dma((nu + 1, GATHER_PIECES)), dma((nu + 1, GATHER_PIECES)),
             dma((nd + 1, GATHER_PIECES)), dma((nd + 1, GATHER_PIECES)),
             dma((n_z, GATHER_PIECES)), dma((n_z, GATHER_PIECES)),

time: 115 us -> 111 us (0.965)
  Pallas kernels: 114 us -> 110 us
    pallas_call x1, Pallas kernels: 112 us -> 107 us  [local(): pl.pallas_call(functools.partial(body, n_ep, n_z, cap), out_shape=(jax.Sh...]
where the time goes in v3:
time: 111 us; the launch traced here: 110 us
  Pallas kernels  110 us (99%)
    pallas_call x1, Pallas kernels, local(): pl.pallas_call(functools.partial(body, n_ep, n_z, cap), out_shape=(jax.Sh...  107 us
    pallas_call x1, Pallas kernels, write_out(): pl.pallas_call(functools.partial(flush, count), out_shape=tuple((jax.Shap...  2.88 us

profile of v3, /device:TPU:1, one launch (start us, length us, event | category | flops | bytes accessed | tf_op | source)
XLA Modules:
  0.0 110.4 jit_solution(18089136480649451466)
XLA Ops:
  0.6 106.7 %shard_map.151 = (bf16[256,2048]{1,0:T(8,128)(2,1)}, bf16[1,2048,128]{2,1,0:T(8,128)(2,1)}, bf16[1,2048,128]{2,1,0:T(8,128)(2,1)}, bf16[1,128,2048]{2,1,0:T(8,12...) custom-call(s32[2,256]{1,0:T(2,128)} %bitcast.5, ...), custom_call_target="tpu_custom_call" | custom-call | tf_op jit(solution)/shard_map/pallas_call | solution.py:660
  107.4 2.9 %shard_map.152 = (bf16[256,2048]{1,0:T(8,128)(2,1)}, bf16[1,2048,128]{2,1,0:T(8,128)(2,1)}, bf16[1,2048,128]{2,1,0:T(8,128)(2,1)}, bf16[1,128,2048]{2,1,0:T(8,12...) custom-call(bf16[256,2048]{1,0:T(8,128)(2,1)} %get-tuple-element.27., ...), custom_call_target="tpu_custom_call" | custom-call | tf_op jit(solution)/shard_map/pallas_call | solution.py:636

commit v4 on v3

--- a/solution.py
+++ b/solution.py
@@ -14,6 +14,12 @@
 SUM_PIECES = 4
 GATHER_PIECES = 2
 CHAIN_CORE = 1
+STRIDE = 2
+NEAR = ((0, 1), (0, 3), (1, 0), (3, 0), (1, 1), (1, 3), (3, 1), (3, 3))
+FAR = (
+    ((0, 2), (1, 2), (3, 2), (2, 2), (2, 0), (2, 1), (2, 3)),
+    ((2, 0), (2, 1), (2, 3), (2, 2), (0, 2), (1, 2), (3, 2)),
+)
 
 
 def plane_peer(e, j, n_ep):
@@ -28,6 +34,10 @@
         y, x = e // 4, e % 4
         return ((y + 4 - j // 4) % 4) * 4 + (x + 4 - j % 4) % 4
     return (e + n_ep - j) % n_ep
+
+
+def shifted(b, dy, dx):
+    return ((b // 4 + dy + 4) % 4) * 4 + (b % 4 + dx + 4) % 4
 
 
 def slot_rows(r, n_ep, cap):
@@ -56,11 +66,11 @@
     tg_out, gg_out, ug_out, dg_out, gn_out, un_out, dn_out, epg_out, gpg_out,
     x, send, rows, wgu, wd, pre, hg, gpu, gput, hidt, prod,
     own, sib_send, sib_recv, dn_send, dn_recv, up_send, up_recv,
-    sc_send, sc_recv, sm, sm_recv, sm_tot, sm_sib, sm_fin,
+    sc_send, sc_recv, sm, sm_recv, sc_sib, sm_sib, sm_fin,
     fin, gat, tg, gg, ug, dg, dnacc,
     ld_sem, wl_sem, loc_sem, in_s, in_r, za_s, za_r, zb_s, zb_r, dx_s, dx_r, dy_s, dy_r,
     sc_s, sc_r, pt_s, pt_r, rd_s, rd_r, ru_s, ru_r, ms_s, ms_r, mx_s, mx_r, mg_s, mg_r,
-    fa_s, fa_r, au_s, au_r, ad_s, ad_r, as_s, as_r, out_sem, met4, met8, pickt,
+    fa_s, fa_r, au_s, au_r, ad_s, ad_r, as_s, as_r, out_sem, met4, met8, pickt, hid,
 ):
     e, tp = lax.axis_index("ep"), lax.axis_index("tp")
     z, c = tp // 2, tp % 2
@@ -177,25 +187,27 @@
         ref = rows.at[arr, pl.ds(other, 2), block(s), :]
         return remote(ref, ref, dy_s.at[s], dy_r.at[s], sibling)
 
-    own_block().start()
-
-    @pl.loop(1, n_ep)
-    def _(j):
-        p = plane_peer(e, j, n_ep)
-        in_copy(p, p, e).start()
-
-    own_block().wait()
-    za_copy(e, mine).start()
-    zb_copy(e, mine).start()
-    dx_copy(e, c).start()
-
-    @pl.loop(1, n_ep)
-    def _(j):
-        s = plane_source(e, j, n_ep)
-        in_copy(s, s, s).wait_recv()
+    def pass_on(s):
         za_copy(s, mine).start()
         zb_copy(s, mine).start()
         dx_copy(s, c).start()
+
+    def exchange(order):
+        for dy, dx in order:
+            p = shifted(e, dy, dx) if n_ep == 16 else (e + dx) % n_ep
+            in_copy(p, p, e).start()
+        own_block().wait()
+        pass_on(e)
+        for dy, dx in order:
+            s = shifted(e, -dy, -dx) if n_ep == 16 else (e - dx + n_ep) % n_ep
+            in_copy(s, s, s).wait_recv()
+            pass_on(s)
+
+    own_block().start()
+    for core in range(2):
+        @pl.when(c == core)
+        def _():
+            exchange(NEAR + FAR[core] if n_ep == 16 else [(0, j) for j in range(1, n_ep)])
 
     def gate_up_part(q):
         pre[...] += jnp.dot(rows[0, q], wgu[q], preferred_element_type=F32)
@@ -253,15 +265,11 @@
         sigma = jax.nn.sigmoid(gate)
         activated = gate * sigma
         derivative = sigma * (1.0 + gate * (1.0 - sigma))
-        hidden = (activated * upv).astype(BF16).astype(F32)
-        gate_pre = (grad * upv * derivative).astype(BF16).astype(F32)
-        up_pre = (grad * activated).astype(BF16).astype(F32)
-        prod[at, :] = hidden * grad
-        gpu[at, :LANES] = gate_pre.astype(BF16)
-        gpu[at, LANES:] = up_pre.astype(BF16)
-        gput[:LANES, at] = gate_pre.T.astype(BF16)
-        gput[LANES:, at] = up_pre.T.astype(BF16)
-        hidt[:, at] = hidden.T.astype(BF16)
+        hidden = (activated * upv).astype(BF16)
+        prod[at, :] = hidden.astype(F32) * grad
+        hid[at, :] = hidden
+        gpu[at, :LANES] = (grad * upv * derivative).astype(BF16)
+        gpu[at, LANES:] = (grad * activated).astype(BF16)
 
     def sc_copy(to, sender):
         return remote(sc_send.at[to], sc_recv.at[sender], sc_s.at[to], sc_r.at[sender], (to, tp))
@@ -291,6 +299,12 @@
                 own[q * qc + i] = part[:, i * LANES : (i + 1) * LANES]
 
     dnacc[...] = jnp.zeros_like(dnacc)
+
+    def turn_piece(source, target):
+        @pl.loop(0, slots // LANES)
+        def _(i):
+            at = pl.ds(pl.multiple_of(i * LANES, LANES), LANES)
+            target[:, at] = source[at, :].astype(F32).T.astype(BF16)
 
     def down_piece(q):
         down = jnp.dot(hidt[...], rows[1, q], preferred_element_type=F32)
@@ -324,13 +338,17 @@
     def ms_copy(o, sender):
         return remote(sm.at[o], sm_recv.at[sender], ms_s.at[o], ms_r.at[sender], at_z(o))
 
-    def mx_copy():
-        return remote(sm_tot, sm_sib, mx_s.at[0], mx_r.at[0], sibling)
+    def hand_copy(i):
+        src, dst = ((sc_send, sc_sib), (sm, sm_sib), (sm_fin, sm_fin))[i]
+        return remote(src, dst, mx_s.at[i], mx_r.at[i], sibling)
 
     def mg_copy(piece, to):
         return remote(sm_fin.at[piece], sm_fin.at[piece], mg_s.at[to], mg_r.at[piece], at_z(to))
 
     score_rows = tok // LANES
+
+    def clear_scores():
+        sm[:, :, 2 * LANES :] = jnp.zeros((n_z, 1, LANES), F32)
 
     def small_start():
         own_scores()
@@ -350,11 +368,14 @@
             column = columns[:cap, s : s + 1]
             for k, slot in enumerate((slot0, slot1)):
                 totals[k] += jnp.sum(jnp.where(here == slot, column, 0.0), axis=0, keepdims=True)
-        sm[:, :, 2 * LANES :] = jnp.zeros((n_z, 1, LANES), F32)
+        clear_scores()
         for k in range(2):
             for h in range(score_rows):
                 sm[k * score_rows + h, :, 2 * LANES :] = totals[k][:, h * LANES : (h + 1) * LANES]
 
+        hand_copy(1).wait_recv()
+        sm[...] += sm_sib[...]
+
         @pl.loop(1, n_z)
         def _(j):
             o = (z + j) % n_z
@@ -367,16 +388,19 @@
             ms_copy(s, s).wait_recv()
 
         sm_recv[z] = sm[z]
-        sm_tot[...] = jnp.sum(sm_recv[...], axis=0)
-        mx_copy().start()
+        sm_fin[z] = jnp.sum(sm_recv[...], axis=0)
+
+        @pl.loop(1, n_z)
+        def _(j):
+            mg_copy(z, (z + j) % n_z).start()
 
     def small_end():
-        mx_copy().wait_recv()
-        sm_fin[z] = sm_tot[...] + sm_sib[...]
-
         @pl.loop(1, n_z)
         def _(j):
-            mg_copy(z, (z + j) % n_z).start()
+            o = (z + j) % n_z
+            mg_copy(o, o).wait_recv()
+
+        hand_copy(2).start()
 
     def scores():
         ones = jnp.ones((8, LANES), F32)
@@ -387,6 +411,10 @@
             )
             sc_send[b, :, :cap] = row[0:1, :]
 
+    def scores_send():
+        hand_copy(0).wait_recv()
+        sc_send[...] += sc_sib[...]
+
         @pl.loop(1, n_ep)
         def _(j):
             p = plane_peer(e, j, n_ep)
@@ -396,11 +424,12 @@
         for copy in grad_stores():
             copy.start()
 
-    work = [scores]
+    work = []
+    work += [functools.partial(turn_piece, hid, hidt), functools.partial(turn_piece, gpu, gput)]
     for q in range(4):
         work += [functools.partial(down_piece, q)]
         work += [functools.partial(in_piece, 0, q), functools.partial(in_piece, 1, q)]
-    work += [small_start, store_start]
+    work += [store_start]
 
     sub = slots // SUM_PIECES
 
@@ -424,14 +453,12 @@
 
     @pl.when(c != CHAIN_CORE)
     def _():
-        for step in work:
+        for step in [scores, scores_send] + work + [small_start, small_middle, small_end]:
             step()
-        small_middle()
-        small_end()
 
     @pl.when(c == CHAIN_CORE)
     def _():
-        todo = work + [pick_piece]
+        todo = [scores, hand_copy(0).start] + work + [clear_scores, hand_copy(1).start, pick_piece]
         for t in range(nd):
             o_dn, o_up = (z + n_z - nd + t) % n_z, (z + nu - t + n_z) % n_z
             pt_copy(o_dn).wait_recv()
@@ -450,13 +477,10 @@
                         total += up_recv[t - 1, part(h), :].astype(F32)
                     up_send[t, part(h), :] = total.astype(BF16)
                     ru_copy(t, h).start()
-                for _ in range(1 if n_z == 16 else len(todo)):
+                for _ in range(min(t, 1) if n_z == 16 else len(todo)):
                     if todo:
                         todo.pop(0)()
-            if t == nd - 2:
-                small_middle()
-
-        small_end()
+
         for h in range(SUM_PIECES):
             total = chip_sum(z, h)
             ru_copy(nu - 1, h).wait_recv()
@@ -480,15 +504,21 @@
 
     def au_copy(t, h, o):
         ref = chunk(o, h)
-        return remote(ref, ref, au_s.at[t, h], au_r.at[t, h], at_z(up_z))
+        hop = 1 if t == 1 else STRIDE
+        return remote(ref, ref, au_s.at[t, h], au_r.at[t, h], at_z((z + hop) % n_z))
 
     def ad_copy(t, h, o):
         ref = chunk(o, h)
-        return remote(ref, ref, ad_s.at[t, h], ad_r.at[t, h], at_z(dn_z))
+        hop = 1 if t == 1 else STRIDE
+        return remote(ref, ref, ad_s.at[t, h], ad_r.at[t, h], at_z((z + n_z - hop) % n_z))
 
     def as_copy(o, h):
         ref = chunk(o, h)
         return remote(ref, ref, as_s.at[o, h], as_r.at[o, h], sibling)
+
+    def store(o):
+        at = pl.ds(pl.multiple_of(o * LANES, LANES), LANES)
+        return pltpu.make_async_copy(tg.at[:, at], tg_out.at[:, at], out_sem.at[3])
 
     @pl.when(c == CHAIN_CORE)
     def _():
@@ -509,27 +539,32 @@
             at = slice(h * piece, (h + 1) * piece)
             acc = jnp.dot(pickt[at, :], gat[...], preferred_element_type=F32)
             tg[at, pl.ds(pl.multiple_of(z * LANES, LANES), LANES)] = acc.astype(BF16)
-            au_copy(1, h, z).start()
-            ad_copy(1, h, z).start()
+            for t in range(1, STRIDE + 1):
+                if t <= nu:
+                    au_copy(t, h, z).start()
+                ad_copy(t, h, z).start()
             as_copy(z, h).start()
+        store(z).start()
         for t in range(1, nd + 1):
             for h in range(GATHER_PIECES):
                 if t <= nu:
                     o = (z + n_z - t) % n_z
                     au_copy(t, h, o).wait_recv()
-                    if t < nu:
-                        au_copy(t + 1, h, o).start()
+                    if t + STRIDE <= nu:
+                        au_copy(t + STRIDE, h, o).start()
                     as_copy(o, h).start()
                 o = (z + t) % n_z
                 ad_copy(t, h, o).wait_recv()
-                if t < nd:
-                    ad_copy(t + 1, h, o).start()
+                if t + STRIDE <= nd:
+                    ad_copy(t + STRIDE, h, o).start()
                 as_copy(o, h).start()
-
-    @pl.loop(1, n_z)
-    def _(j):
-        o = (z + j) % n_z
-        mg_copy(o, o).wait_recv()
+            if t <= nu:
+                store((z + n_z - t) % n_z).start()
+            store((z + t) % n_z).start()
+
+    @pl.when(c == CHAIN_CORE)
+    def _():
+        hand_copy(2).wait_recv()
 
     units = float(LANES * 2 * n_z)
     for o in range(n_z):
@@ -553,12 +588,11 @@
     @pl.when(c != CHAIN_CORE)
     def _():
         @pl.loop(0, n_z)
-        def _(o):
+        def _(j):
+            o = (z + n_z + (j % 2) * j - j // 2) % n_z
             for h in range(GATHER_PIECES):
                 as_copy(o, h).wait_recv()
-
-    tg_store = pltpu.make_async_copy(tg, tg_out, out_sem.at[3])
-    tg_store.start()
+            store(o).start()
 
     for copy in grad_stores():
         copy.wait()
@@ -567,7 +601,6 @@
     def _(j):
         p = plane_peer(e, j, n_ep)
         in_copy(p, p, e).wait_send()
-        sc_copy(p, e).wait_send()
 
     @pl.loop(0, n_ep)
     def _(s):
@@ -576,21 +609,29 @@
         dx_copy(s, c).wait_send()
         dy_copy(s, c).wait_send()
 
-    @pl.loop(1, n_z)
-    def _(j):
-        o = (z + j) % n_z
-        ms_copy(o, z).wait_send()
-        mg_copy(z, o).wait_send()
-
-    mx_copy().wait_send()
     @pl.when(c != CHAIN_CORE)
     def _():
+        @pl.loop(1, n_ep)
+        def _(j):
+            sc_copy(plane_peer(e, j, n_ep), e).wait_send()
+
+        @pl.loop(1, n_z)
+        def _(j):
+            o = (z + j) % n_z
+            ms_copy(o, z).wait_send()
+            mg_copy(z, o).wait_send()
+
+        hand_copy(2).wait_send()
+
         @pl.loop(0, n_z)
         def _(o):
             pt_copy(o).wait_send()
 
     @pl.when(c == CHAIN_CORE)
     def _():
+        hand_copy(0).wait_send()
+        hand_copy(1).wait_send()
+
         @pl.loop(1, n_ep)
         def _(j):
             fa_copy(plane_peer(e, j, n_ep), e).wait_send()
@@ -613,19 +654,29 @@
             def _(o):
                 as_copy(o, h).wait_send()
 
-    tg_store.wait()
+    pltpu.make_async_copy(tg, tg_out, out_sem.at[3]).wait()
 
 
 def flush(count, *refs):
     ins, outs, bufs = refs[:count], refs[count : 2 * count], refs[2 * count : 3 * count]
     in_sem, out_sem = refs[3 * count :]
-    reads = [pltpu.make_async_copy(ins[i], bufs[i], in_sem.at[i]) for i in range(count)]
-    writes = [pltpu.make_async_copy(bufs[i], outs[i], out_sem.at[i]) for i in range(count)]
+    reads, writes = [], []
+    for i in range(count):
+        rows = ins[i].shape[-2]
+        pieces = 4 if rows % 64 == 0 else 1
+        for p in range(pieces):
+            at = pl.ds(p * (rows // pieces), rows // pieces)
+            src, buf, dst = (
+                (ref.at[at, :] if len(ref.shape) == 2 else ref.at[:, at, :])
+                for ref in (ins[i], bufs[i], outs[i])
+            )
+            reads.append(pltpu.make_async_copy(src, buf, in_sem.at[i, p]))
+            writes.append(pltpu.make_async_copy(buf, dst, out_sem.at[i, p]))
     for copy in reads:
         copy.start()
-    for i in range(count):
-        reads[i].wait()
-        writes[i].start()
+    for read, write in zip(reads, writes):
+        read.wait()
+        write.start()
     for copy in writes:
         copy.wait()
 
@@ -639,7 +690,7 @@
         in_specs=[any_spec] * count,
         out_specs=(any_spec,) * count,
         scratch_shapes=[pltpu.VMEM(a.shape, a.dtype) for a in arrays]
-        + [pltpu.SemaphoreType.DMA((count,)), pltpu.SemaphoreType.DMA((count,))],
+        + [pltpu.SemaphoreType.DMA((count, 4)), pltpu.SemaphoreType.DMA((count, 4))],
     )(*arrays)
 
 
@@ -695,8 +746,8 @@
             vm((n_ep, 1, scw), F32),
             vm((n_z, 1, 3 * LANES), F32),
             vm((n_z, 1, 3 * LANES), F32),
-            vm((1, 3 * LANES), F32),
-            vm((1, 3 * LANES), F32),
+            vm((n_ep, 1, scw), F32),
+            vm((n_z, 1, 3 * LANES), F32),
             vm((n_z, 1, 3 * LANES), F32),
             vm((slots, LANES), BF16),
             vm((slots, LANES), BF16),
@@ -711,13 +762,14 @@
             dma((n_ep,)), dma((n_ep,)),
             dma((n_z,)), dma((n_z,)),
             dma((nd, SUM_PIECES)), dma((nd, SUM_PIECES)), dma((nu, SUM_PIECES)), dma((nu, SUM_PIECES)),
-            dma((n_z,)), dma((n_z,)), dma((1,)), dma((1,)), dma((n_z,)), dma((n_z,)),
+            dma((n_z,)), dma((n_z,)), dma((3,)), dma((3,)), dma((n_z,)), dma((n_z,)),
             dma((n_ep,)), dma((n_ep,)),
             dma((nu + 1, GATHER_PIECES)), dma((nu + 1, GATHER_PIECES)),
             dma((nd + 1, GATHER_PIECES)), dma((nd + 1, GATHER_PIECES)),
             dma((n_z, GATHER_PIECES)), dma((n_z, GATHER_PIECES)),
             dma((4,)), pltpu.SemaphoreType.REGULAR, pltpu.SemaphoreType.REGULAR,
             vm((tok, slots), BF16),
+            vm((slots, unit), BF16),
         ],
         compiler_params=pltpu.CompilerParams(
             collective_id=0, has_side_effects=True, vmem_limit_bytes=56 * 1024 * 1024

time: 111 us -> 103 us (0.928)
  Pallas kernels: 110 us -> 102 us
    pallas_call x1, Pallas kernels: 107 us -> 99.3 us  [local(): pl.pallas_call(functools.partial(body, n_ep, n_z, cap), out_shape=(jax.Sh...]
where the time goes in v4:
time: 103 us
  Pallas kernels  102 us (99%)
    pallas_call x1, Pallas kernels, local(): pl.pallas_call(functools.partial(body, n_ep, n_z, cap), out_shape=(jax.Sh...  99.3 us
    pallas_call x1, Pallas kernels, write_out(): pl.pallas_call(functools.partial(flush, count), out_shape=tuple((jax.Shap...  3.08 us

profile of v4, /device:TPU:1, one launch (start us, length us, event | category | flops | bytes accessed | tf_op | source)
XLA Modules:
  0.0 103.2 jit_solution(14878102353368655079)
XLA Ops:
  0.6 99.3 %shard_map.151 = (bf16[256,2048]{1,0:T(8,128)(2,1)}, bf16[1,2048,128]{2,1,0:T(8,128)(2,1)}, bf16[1,2048,128]{2,1,0:T(8,128)(2,1)}, bf16[1,128,2048]{2,1,0:T(8,12...) custom-call(s32[2,256]{1,0:T(2,128)} %bitcast.5, ...), custom_call_target="tpu_custom_call" | custom-call | tf_op jit(solution)/shard_map/pallas_call | solution.py:711
  100.0 3.1 %shard_map.152 = (bf16[256,2048]{1,0:T(8,128)(2,1)}, bf16[1,2048,128]{2,1,0:T(8,128)(2,1)}, bf16[1,2048,128]{2,1,0:T(8,128)(2,1)}, bf16[1,128,2048]{2,1,0:T(8,12...) custom-call(bf16[256,2048]{1,0:T(8,128)(2,1)} %get-tuple-element.27., ...), custom_call_target="tpu_custom_call" | custom-call | tf_op jit(solution)/shard_map/pallas_call | solution.py:687

commit v5 on v4

--- a/solution.py
+++ b/solution.py
@@ -402,9 +402,9 @@
 
         hand_copy(2).start()
 
-    def scores():
+    def scores(first=0, last=n_ep):
         ones = jnp.ones((8, LANES), F32)
-        for b in range(n_ep):
+        for b in range(first, last):
             row = lax.dot_general(
                 ones, prod[b * cap : (b + 1) * cap, :], CONTRACT_LAST,
                 precision=lax.Precision.HIGHEST, preferred_element_type=F32,
@@ -458,7 +458,8 @@
 
     @pl.when(c == CHAIN_CORE)
     def _():
-        todo = [scores, hand_copy(0).start] + work + [clear_scores, hand_copy(1).start, pick_piece]
+        pieces = [functools.partial(scores, b, b + 2) for b in range(0, n_ep, 2)]
+        todo = pieces + [hand_copy(0).start] + work + [clear_scores, hand_copy(1).start, pick_piece]
         for t in range(nd):
             o_dn, o_up = (z + n_z - nd + t) % n_z, (z + nu - t + n_z) % n_z
             pt_copy(o_dn).wait_recv()

time: 103 us -> 103 us (level)
  no operation moved by 1% of the time
where the time goes in v5:
time: 103 us
  Pallas kernels  102 us (99%)
    pallas_call x1, Pallas kernels, local(): pl.pallas_call(functools.partial(body, n_ep, n_z, cap), out_shape=(jax.Sh...  99.4 us
    pallas_call x1, Pallas kernels, write_out(): pl.pallas_call(functools.partial(flush, count), out_shape=tuple((jax.Shap...  3.08 us

profile of v5, /device:TPU:1, one launch (start us, length us, event | category | flops | bytes accessed | tf_op | source)
XLA Modules:
  0.0 103.3 jit_solution(13058749358941207071)
XLA Ops:
  0.6 99.4 %shard_map.151 = (bf16[256,2048]{1,0:T(8,128)(2,1)}, bf16[1,2048,128]{2,1,0:T(8,128)(2,1)}, bf16[1,2048,128]{2,1,0:T(8,128)(2,1)}, bf16[1,128,2048]{2,1,0:T(8,12...) custom-call(s32[2,256]{1,0:T(2,128)} %bitcast.5, ...), custom_call_target="tpu_custom_call" | custom-call | tf_op jit(solution)/shard_map/pallas_call | solution.py:712
  100.0 3.1 %shard_map.152 = (bf16[256,2048]{1,0:T(8,128)(2,1)}, bf16[1,2048,128]{2,1,0:T(8,128)(2,1)}, bf16[1,2048,128]{2,1,0:T(8,128)(2,1)}, bf16[1,128,2048]{2,1,0:T(8,12...) custom-call(bf16[256,2048]{1,0:T(8,128)(2,1)} %get-tuple-element.27., ...), custom_call_target="tpu_custom_call" | custom-call | tf_op jit(solution)/shard_map/pallas_call | solution.py:688
